TPU v7x, 32 devices: a whole 2x2x4 slice. The times are simulated.
32 devices in a mesh: sp: 16 (over z, y, x), tp: 2 (over core).
Axes of the slice: x: 2, y: 2, z: 4, core: 2. Of those that a mesh axis runs over, the one named last changes fastest.
Arguments:
- query_one: bfloat16 [2048, 1024], P('sp', 'tp'), may hold values from -85 to 85
- key_one: bfloat16 [2048, 1024], P('sp', 'tp'), may hold values from -6.5 to 6.5
- query_two: bfloat16 [2048, 1024], P('sp', 'tp'), may hold values from -85 to 85
- key_two: bfloat16 [2048, 1024], P('sp', 'tp'), may hold values from -6.5 to 6.5
- values: bfloat16 [2048, 2048], P('sp', 'tp'), may hold values from -6 to 6
- mix_weight: float32 [8], P('tp'), may hold values from 0.3 to 0.8
- head_gain: float32 [256], replicated, may hold values from 0.1 to 1.9
- residual: bfloat16 [2048, 2048], P(('sp', 'tp')), may hold values from -6 to 6
- out_weight: bfloat16 [2048, 2048], P('tp'), may hold values from -0.125 to 0.125
- norm_gain: float32 [2048], replicated, may hold values from 0.1 to 1.9
- lift_weight: bfloat16 [2048, 5632], P('sp', 'tp'), may hold values from -0.125 to 0.125
- gate_weight: bfloat16 [2048, 5632], P('sp', 'tp'), may hold values from -0.125 to 0.125
- conv_taps: float32 [3, 5632], P(None, 'tp'), may hold values from -3 to 3
- down_weight: bfloat16 [5632, 2048], P('tp'), may hold values from -0.078125 to 0.078125
Outputs:
- layer_out: bfloat16 [2048, 2048], P(('sp', 'tp'))
All inputs are finite; a program needn't handle non-finite values.
Results may differ from a plain program's by a relative error of at most 0.015.
Values may be sent and summed in bfloat16 or wider, within the bound.
A program may use at most 128 MiB of HBM per device.

v0:
```python
import jax
import jax.numpy as jnp
from jax import lax
from jax.sharding import PartitionSpec as P

HD = 128
STRETCH = 64
WIDTH = 3


epsilon = 1e-06
masked_score = -1e30


def passed_along(block, axis, distance):
    devices = range(lax.axis_size(axis))
    route = [(i - distance, i) for i in devices if i - distance in devices]
    return lax.ppermute(block, axis, route)


def update_map(peak, total, acc, queries, keys, vals, visible):
    scores = jnp.einsum("thd,shd->hts", queries, keys, preferred_element_type=jnp.float32) * HD ** (
        -0.5
    )
    scores = jnp.where(visible[None], scores, masked_score)
    new_peak = jnp.maximum(peak, jnp.max(scores, axis=-1))
    weights = jnp.where(visible[None], jnp.exp(scores - new_peak[..., None]), 0.0)
    total = jnp.sum(weights, axis=-1)
    acc = jnp.einsum(
        "hts,she->hte", weights.astype(jnp.bfloat16), vals, preferred_element_type=jnp.float32
    )
    return (new_peak, total, acc)


def on_device(
    query_one,
    key_one,
    query_two,
    key_two,
    values,
    mix_weight,
    head_gain,
    residual,
    out_weight,
    norm_gain,
    lift_weight,
    gate_weight,
    conv_taps,
    down_weight,
):
    tok_local = query_one.shape[0]
    heads_local = mix_weight.shape[0]
    val_width = values.shape[1] // heads_local
    model_width = residual.shape[1]
    offset = lax.axis_index("sp") * tok_local
    q_pos = offset + lax.iota(jnp.int32, tok_local)
    q_one = query_one.reshape(tok_local, heads_local, HD)
    q_two = query_two.reshape(tok_local, heads_local, HD)
    start_peak = jnp.full((heads_local, tok_local), masked_score, jnp.float32)
    start_total = jnp.zeros((heads_local, tok_local), jnp.float32)
    start_acc = jnp.zeros((heads_local, tok_local, val_width), jnp.float32)
    initial = (start_peak, start_total, start_acc, start_peak, start_total, start_acc)
    first_keys = lax.all_gather(key_one, "sp", axis=0, tiled=True)
    second_keys = lax.all_gather(key_two, "sp", axis=0, tiled=True)
    piece_vals = lax.all_gather(values, "sp", axis=0, tiled=True)
    count = first_keys.shape[0]
    k_pos = lax.iota(jnp.int32, count)
    visible = k_pos[None, :] // STRETCH <= q_pos[:, None] // STRETCH
    first_keys = first_keys.reshape(count, heads_local, HD)
    second_keys = second_keys.reshape(count, heads_local, HD)
    piece_vals = piece_vals.reshape(count, heads_local, val_width)
    first = update_map(initial[0], initial[1], initial[2], q_one, first_keys, piece_vals, visible)
    second = update_map(initial[3], initial[4], initial[5], q_two, second_keys, piece_vals, visible)
    state = first + second
    mixed = (
        state[2] / state[1][..., None] - mix_weight[:, None, None] * state[5] / state[4][..., None]
    )
    head_out = (
        mixed * lax.rsqrt(jnp.mean(mixed * mixed, axis=-1, keepdims=True) + epsilon) * head_gain
    ).astype(jnp.bfloat16)
    out_heads = out_weight.reshape(heads_local, val_width, model_width)
    piece = head_out
    attended = lax.psum_scatter(
        jnp.einsum("hte,hed->td", piece, out_heads, preferred_element_type=jnp.float32).astype(
            jnp.bfloat16
        ),
        "tp",
        scatter_dimension=0,
        tiled=True,
    ).astype(jnp.float32)
    stream = residual.astype(jnp.float32) + attended
    normed = (
        stream * lax.rsqrt(jnp.mean(stream * stream, axis=-1, keepdims=True) + epsilon) * norm_gain
    ).astype(jnp.bfloat16)
    whole_rows = lax.all_gather(normed, "tp", axis=0, tiled=True)
    lift_pre = jnp.dot(
        whole_rows,
        lax.all_gather(lift_weight, "sp", axis=0, tiled=True),
        preferred_element_type=jnp.float32,
    )
    gate_pre = jnp.dot(
        whole_rows,
        lax.all_gather(gate_weight, "sp", axis=0, tiled=True),
        preferred_element_type=jnp.float32,
    )
    lifted = lift_pre.astype(jnp.bfloat16)
    gated = gate_pre.astype(jnp.bfloat16)
    prior = passed_along(gated[tok_local - (WIDTH - 1) :], "sp", 1)
    extended = jnp.concatenate([prior, gated], axis=0).astype(jnp.float32)
    conv = conv_taps[0] * extended[0:tok_local]
    for index in range(1, WIDTH):
        conv = conv + conv_taps[index] * extended[index : index + tok_local]
    hidden = (jax.nn.silu(conv) * lifted.astype(jnp.float32)).astype(jnp.bfloat16)
    piece = hidden
    mixer = lax.psum_scatter(
        jnp.dot(piece, down_weight, preferred_element_type=jnp.float32).astype(jnp.bfloat16),
        "tp",
        scatter_dimension=0,
        tiled=True,
    ).astype(jnp.float32)
    return (stream + mixer).astype(jnp.bfloat16)


def solution(mesh):
    return jax.shard_map(
        on_device,
        mesh=mesh,
        in_specs=(
            P("sp", "tp"),
            P("sp", "tp"),
            P("sp", "tp"),
            P("sp", "tp"),
            P("sp", "tp"),
            P("tp"),
            P(),
            P(("sp", "tp"), None),
            P("tp", None),
            P(),
            P("sp", "tp"),
            P("sp", "tp"),
            P(None, "tp"),
            P("tp", None),
        ),
        out_specs=P(("sp", "tp"), None),
        check_vma=False,
    )
```

profile of v0, /device:TPU:25, one launch (start us, length us, event | category | flops | bytes accessed | tf_op | source)
XLA Modules:
  0.0 558.7 jit_solution(8064380941577082344)
XLA Ops:
  6.5 1.7 copy.17
  8.3 1.7 copy.22
  10.0 0.0 all-gather.8.cloned.1.call-start
  10.0 1.8 copy.20
  11.9 0.2 broadcast_compare_fusion
  12.2 60.0 %all-gather.6.cloned.1.call-done = bf16[2048,512]{0,1:T(8,128)(2,1)} async-done(((bf16[128,512]{0,1:T(8,128)(2,1)}), bf16[2048,512]{0,1:T(8,128)(2,1)}) %all-gather.6.cloned.1.call-update) | async-done | bytes 2097168 | tf_op jit(solution)/shard_map/all_gather | solution.py:63
  72.2 4.7 fusion
  76.8 59.2 %all-gather.10.cloned.1.call-done = bf16[2048,512]{0,1:T(8,128)(2,1)} async-done(((bf16[128,512]{0,1:T(8,128)(2,1)}), bf16[2048,512]{0,1:T(8,128)(2,1)}) %all-gather.10.cloned.1.call-update) | async-done | bytes 2097168 | tf_op jit(solution)/shard_map/all_gather | solution.py:64
  136.0 5.1 fusion.5
  141.1 1.9 copy-done.3
  143.1 1.3 fusion.7
  144.3 81.3 %all-gather.8.cloned.1.call-done = bf16[2048,1024]{0,1:T(8,128)(2,1)} async-done(((bf16[128,1024]{0,1:T(8,128)(2,1)}), bf16[2048,1024]{0,1:T(8,128)(2,1)}) %all-gather.8.cloned.1.call-update) | async-done | bytes 4194320 | tf_op jit(solution)/shard_map/all_gather | solution.py:65
  225.7 5.5 fusion.35
  231.1 0.4 copy-done.9
  231.6 2.1 multiply_reduce_fusion.1
  233.8 1.6 fusion.9
  235.4 0.5 all-gather.12.cloned.1.call-update
  236.0 0.5 all-gather.14.cloned.1.call-update
  236.6 7.6 %reduce-scatter.3.cloned.1.call-done = bf16[64,2048]{1,0:T(8,128)(2,1)} async-done(((bf16[128,2048]{1,0:T(8,128)(2,1)}), bf16[64,2048]{1,0:T(8,128)(2,1)}) %reduce-scatter.3.cloned.1.call-update) | async-done | bytes 262160 | tf_op jit(solution)/shard_map/reduce_scatter | solution.py:83
  244.2 1.1 multiply_reduce_fusion
  245.4 1.1 multiply_convert_fusion
  246.5 2.2 all_gather.21
  248.6 138.2 %all-gather.12.cloned.1.call-done = bf16[2048,2816]{1,0:T(8,128)(2,1)} async-done(((bf16[128,2816]{1,0:T(8,128)(2,1)}), bf16[2048,2816]{1,0:T(8,128)(2,1)}) %all-gather.12.cloned.1.call-update) | async-done | bytes 11534352 | tf_op jit(solution)/shard_map/all_gather | solution.py:103
  386.8 5.9 %convolution_convert_fusion.1 = bf16[128,2816]{1,0:T(8,128)(2,1)S(1)} fusion(bf16[128,2048]{1,0:T(8,128)(2,1)S(1)} %all_gather.21, bf16[2048,2816]{1,0:T(8,128)(2,1)} %all-gather.12.cloned.1.call-done), kind=kOutput, calls=%fused_computation.10 | convolution fusion | flops 1476755456 | bytes 12779520 | tf_op jit(solution)/shard_map/dot_general | solution.py:101
  392.8 3.1 collective-permute-start
  395.9 0.1 slice_reduce_fusion.2
  396.0 3.0 collective-permute-done
  399.0 0.2 maximum_convert_fusion
  399.2 129.9 %all-gather.14.cloned.1.call-done = bf16[2048,2816]{1,0:T(8,128)(2,1)} async-done(((bf16[128,2816]{1,0:T(8,128)(2,1)}), bf16[2048,2816]{1,0:T(8,128)(2,1)}) %all-gather.14.cloned.1.call-update) | async-done | bytes 11534352 | tf_op jit(solution)/shard_map/all_gather | solution.py:98
  529.1 12.1 %convolution_convert_fusion.2 = bf16[128,2048]{1,0:T(8,128)(2,1)} fusion(bf16[2816,2048]{1,0:T(8,128)(2,1)} %param.27, bf16[128,2048]{1,0:T(8,128)(2,1)S(1)} %all_gather.21, bf16[2048,2816]{1,0:T(8,128)(2,1)} %all-gather.14.cloned.1.call-done, f32[130,2816]{1,0:T(8,128)S(1)} %maximum_convert_fusion, f32[2816]{0:T(1024)S(1)} %get-tuple-element.8, ...), kind=kOutput, calls=%fused_computation.17 | convolution fusion | flops 2957737984 | bytes 28479488 | tf_op jit(solution)/shard_map/dot_general | solution.py:116
  541.3 8.8 %reduce-scatter.5.cloned.1.call-done = bf16[64,2048]{1,0:T(8,128)(2,1)} async-done(((bf16[128,2048]{1,0:T(8,128)(2,1)}), bf16[64,2048]{1,0:T(8,128)(2,1)}) %reduce-scatter.5.cloned.1.call-update) | async-done | bytes 262160 | tf_op jit(solution)/shard_map/reduce_scatter | solution.py:115
  550.1 1.7 add_convert_fusion
  (38 shorter events, 0.4 us)
Async XLA Ops:
  6.5 129.5 %copy-start = (bf16[128,512]{1,0:T(8,128)(2,1)S(1)}, bf16[128,512]{1,0:T(8,128)(2,1)}, u32[]{:S(2)}) copy-start(bf16[128,512]{1,0:T(8,128)(2,1)} %param.16) | copy-start | bytes 393220
  6.5 65.6 %all-gather.6.cloned.1.call-start = ((), (), s32[]{:S(2)}) async-start(), calls=%async_computation.2 | async-start | bytes 2228224 | tf_op jit(solution)/shard_map/all_gather | solution.py:63
  8.3 127.8 %all-gather.10.cloned.1.call-start = ((), (), s32[]{:S(2)}) async-start(), calls=%async_computation.4 | async-start | bytes 2228224 | tf_op jit(solution)/shard_map/all_gather | solution.py:64
  10.0 215.7 %all-gather.8.cloned.1.call-start = ((), (), s32[]{:S(2)}) async-start(), calls=%async_computation.3 | async-start | bytes 4456448 | tf_op jit(solution)/shard_map/all_gather | solution.py:65
  11.9 232.4 %reduce-scatter.3.cloned.1.call-start = ((), (), s32[]{:S(2)}) async-start(), calls=%async_computation.5 | async-start | bytes 786432 | tf_op jit(solution)/shard_map/reduce_scatter | solution.py:83
  141.1 1.9 copy-start.3
  141.1 84.5 %copy-start.10 = (f32[4]{0:T(128)S(1)}, f32[4]{0:T(128)}, u32[]{:S(2)}) copy-start(f32[4]{0:T(128)} %param.19) | copy-start | bytes 52
  225.7 5.5 copy-start.2
  225.7 5.9 %copy-start.9 = (bf16[2048,1024]{0,1:T(8,128)(2,1)S(1)}, bf16[2048,1024]{0,1:T(8,128)(2,1)}, u32[]{:S(2)}) copy-start(bf16[2048,1024]{0,1:T(8,128)(2,1)} %all-gather.8.cloned.1.call-done) | copy-start | bytes 12582916
  231.6 2.2 copy-start.1
  231.6 2.2 copy-start.8
  233.8 10.5 %copy-start.4 = (bf16[64,2048]{1,0:T(8,128)(2,1)S(1)}, bf16[64,2048]{1,0:T(8,128)(2,1)}, u32[]{:S(2)}) copy-start(bf16[64,2048]{1,0:T(8,128)(2,1)} %param.21) | copy-start | bytes 786436
  233.8 11.6 %copy-start.7 = (f32[2048]{0:T(1024)S(1)}, f32[2048]{0:T(1024)}, u32[]{:S(2)}) copy-start(f32[2048]{0:T(1024)} %param.23) | copy-start | bytes 24580
  235.4 151.4 %all-gather.12.cloned.1.call-start = ((), (), s32[]{:S(2)}) async-start(), calls=%async_computation.6 | async-start | bytes 12255232 | tf_op jit(solution)/shard_map/all_gather | solution.py:103
  236.0 293.1 %all-gather.14.cloned.1.call-start = ((), (), s32[]{:S(2)}) async-start(), calls=%async_computation.7 | async-start | bytes 12255232 | tf_op jit(solution)/shard_map/all_gather | solution.py:98
  236.6 313.5 %reduce-scatter.5.cloned.1.call-start = ((), (), s32[]{:S(2)}) async-start(), calls=%async_computation.8 | async-start | bytes 786432 | tf_op jit(solution)/shard_map/reduce_scatter | solution.py:115
  248.6 147.3 %copy-start.6 = (f32[3,2816]{1,0:T(4,128)S(1)}, f32[3,2816]{1,0:T(4,128)}, u32[]{:S(2)}) copy-start(f32[3,2816]{1,0:T(4,128)} %param.26) | copy-start | bytes 101380
  392.8 6.2 %collective-permute-start = (bf16[2,2816]{1,0:T(2,128)(2,1)S(1)}, bf16[2,2816]{1,0:T(2,128)(2,1)S(1)}, u32[]{:S(2)}, u32[]{:S(2)}) collective-permute-start(bf16[2,2816]{1,0:T(2,128)(2,1)S(1)} %slice.28), channel_id=1, source_target_pairs={{0,2},{2,4},{4,6},{6,8},{8,10},{10,12},{12,14},{14,16},{16,18},{18... | collective-permute-start | bytes 33800 | tf_op jit(solution)/shard_map/ppermute | solution.py:18
  529.1 21.0 %copy-start.5 = (bf16[64,2048]{1,0:T(8,128)(2,1)S(1)}, bf16[64,2048]{1,0:T(8,128)(2,1)}, u32[]{:S(2)}) copy-start(bf16[64,2048]{1,0:T(8,128)(2,1)} %reduce-scatter.3.cloned.1.call-done) | copy-start | bytes 786436
Sparse Core Ops, SparseCore 0:
  10.0 62.0 all-gather.5
  74.9 61.1 all-gather.9
  138.7 86.8 all-gather.7
  235.5 8.6 reduce-scatter.2
  246.8 139.9 all-gather.11
  389.4 139.5 all-gather.13
  541.4 8.6 reduce-scatter.4
where the time goes:
time: 560 us; the launch traced here: 559 us
  waiting for transfers between devices  489 us (87%)
  matrix products  37 us (7%)
  between operations  13.6 us (2%)
  local copies, waits for them, and re-layouts  7.67 us (1%)
  other arithmetic  5.62 us (1%)
    all_gather x1, waiting for transfers between devices, on_device(): lax.all_gather(gate_weight, 'sp', axis=0, tiled=True)  138 us
    all_gather x1, waiting for transfers between devices, on_device(): lax.all_gather(lift_weight, 'sp', axis=0, tiled=True)  130 us
    all_gather x1, waiting for transfers between devices, on_device(): piece_vals = lax.all_gather(values, 'sp', axis=0, tiled=True)  81.3 us
    all_gather x1, waiting for transfers between devices, on_device(): first_keys = lax.all_gather(key_one, 'sp', axis=0, tiled=True)  60 us
    all_gather x1, waiting for transfers between devices, on_device(): second_keys = lax.all_gather(key_two, 'sp', axis=0, tiled=True)  59.2 us
    dot_general x1, matrix products, on_device(): jnp.dot(piece, down_weight, preferred_element_type=jnp.float32)  12.1 us
  transfers between devices with their start and end apart: 8, of which 8 were waited for; matrix products, arithmetic and copies ran while one was open for 4% of the time, Pallas kernels for 0%

commit v1 on v0

--- a/solution.py
+++ b/solution.py
@@ -1,6 +1,10 @@
+import functools
+
 import jax
 import jax.numpy as jnp
 from jax import lax
+from jax.experimental import pallas as pl
+from jax.experimental.pallas import tpu as pltpu
 from jax.sharding import PartitionSpec as P
 
 HD = 128
@@ -120,10 +124,450 @@
     ).astype(jnp.float32)
     return (stream + mixer).astype(jnp.bfloat16)
 
+MESH = pl.DeviceIdType.MESH
+
+
+def remote(src, dst, send_sem, recv_sem, sp, tp):
+    return pltpu.make_async_remote_copy(
+        src_ref=src,
+        dst_ref=dst,
+        send_sem=send_sem,
+        recv_sem=recv_sem,
+        device_id=(sp, tp),
+        device_id_type=MESH,
+    )
+
+
+def greet(peers, count=None):
+    barrier = pltpu.get_barrier_semaphore()
+    for peer in peers:
+        pl.semaphore_signal(barrier, inc=1, device_id=peer, device_id_type=MESH)
+    pl.semaphore_wait(barrier, len(peers) if count is None else count)
+
+
+def block_of(index, size):
+    return pl.ds(pl.multiple_of(index * size, size), size)
+
+
+def spread_kernel(
+    plane, planes, width, q1, k1, q2, k2, v, lift, gate,
+    q_all, kv_all, lift_all, gate_all,
+    own_sem, a_send, a_recv, w_send, w_recv, kv_send, kv_recv, g_send, g_recv,
+):
+    sp, tp = lax.axis_index("sp"), lax.axis_index("tp")
+    z, p = sp // plane, sp % plane
+    tok = q1.shape[0]
+    tiles = lift.shape[1] // 128
+    greet(
+        [(z * plane + (p + d) % plane, tp) for d in range(1, plane)]
+        + [((z + d) % planes * plane + p, tp) for d in range(1, planes)]
+    )
+
+    def piece(head, row):
+        h1, h2 = block_of(head, HD), block_of(head, 2 * HD)
+        rows, all_rows = block_of(row % plane, tok), block_of(row, tok)
+        return [
+            (q1.at[:, h1], q_all.at[rows, 0:HD]),
+            (q2.at[:, h1], q_all.at[rows, HD : 2 * HD]),
+            (k1.at[:, h1], kv_all.at[all_rows, 0:HD]),
+            (k2.at[:, h1], kv_all.at[all_rows, HD : 2 * HD]),
+            (v.at[:, h2], kv_all.at[all_rows, 2 * HD : 4 * HD]),
+        ]
+
+    def units(index):
+        return pl.ds(pl.multiple_of(index * tiles // planes * 128, 128), width)
+
+    started = []
+    own = []
+    for n, (src, dst) in enumerate(piece(p, sp)):
+        own.append(pltpu.make_async_copy(src, dst, own_sem.at[n]))
+    for m, (src, dst) in enumerate(((lift, lift_all), (gate, gate_all))):
+        own.append(
+            pltpu.make_async_copy(src.at[:, units(z)], dst.at[block_of(sp, tok), :], own_sem.at[5 + m])
+        )
+    for copy in own:
+        copy.start()
+    for d in range(1, plane):
+        there = (p + d) % plane
+        for n, (src, dst) in enumerate(piece(there, sp)):
+            copy = remote(src, dst, a_send.at[d, n], a_recv.at[d, n], z * plane + there, tp)
+            copy.start()
+            started.append(copy)
+    for d in range(1, planes):
+        there = (z + d) % planes
+        for m, (src, dst) in enumerate(((lift, lift_all), (gate, gate_all))):
+            copy = remote(
+                src.at[:, units(there)], dst.at[block_of(sp, tok), :],
+                w_send.at[d, m], w_recv.at[d, m], there * plane + p, tp,
+            )
+            copy.start()
+            started.append(copy)
+    for m, (src, dst) in enumerate(((lift, lift_all), (gate, gate_all))):
+        for e in range(1, plane):
+            copy = remote(
+                src.at[:, units(z)], dst.at[block_of(sp, tok), :],
+                g_send.at[0, e, m], g_recv.at[0, e, m], z * plane + (p + e) % plane, tp,
+            )
+            copy.start()
+            started.append(copy)
+    for copy in own:
+        copy.wait()
+    for d in range(1, plane):
+        source = z * plane + (p + plane - d) % plane
+        for n, (src, dst) in enumerate(piece(p, source)):
+            remote(src, dst, a_send.at[d, n], a_recv.at[d, n], source, tp).wait_recv()
+    mine = kv_all.at[block_of(z, plane * tok), :]
+    for d in range(1, planes):
+
+        @pl.when(z + d < planes)
+        def _():
+            remote(mine, mine, kv_send.at[d], kv_recv.at[d], (z + d) % planes * plane + p, tp).start()
+
+    for d in range(1, planes):
+        source = (z + planes - d) % planes * plane + p
+        rows = block_of(source, tok)
+        for m, dst in enumerate((lift_all, gate_all)):
+            remote(dst.at[rows, :], dst.at[rows, :], w_send.at[d, m], w_recv.at[d, m], source, tp).wait_recv()
+            for e in range(1, plane):
+                copy = remote(
+                    dst.at[rows, :], dst.at[rows, :],
+                    g_send.at[d, e, m], g_recv.at[d, e, m], z * plane + (p + e) % plane, tp,
+                )
+                copy.start()
+                started.append(copy)
+    for d in range(planes):
+        for e in range(1, plane):
+            there = (p + plane - e) % plane
+            rows = block_of((z + planes - d) % planes * plane + there, tok)
+            for m, dst in enumerate((lift_all, gate_all)):
+                remote(
+                    dst.at[rows, :], dst.at[rows, :], g_send.at[d, e, m], g_recv.at[d, e, m],
+                    z * plane + there, tp,
+                ).wait_recv()
+    for d in range(1, planes):
+        below = kv_all.at[block_of((z + planes - d) % planes, plane * tok), :]
+
+        @pl.when(z - d >= 0)
+        def _():
+            remote(below, below, kv_send.at[d], kv_recv.at[d], sp, tp).wait_recv()
+
+        @pl.when(z + d < planes)
+        def _():
+            remote(mine, mine, kv_send.at[d], kv_recv.at[d], sp, tp).wait_send()
+
+    for copy in started:
+        copy.wait_send()
+
+
+def out_kernel(
+    plane, planes, head_out, out_weight, residual, gain,
+    normed, halo, stream,
+    heads, part, part_in, tail, own_sem, a_send, a_recv, t_send, t_recv,
+    z_send, z_recv, f_send, f_recv, h_send, h_recv,
+):
+    sp, tp = lax.axis_index("sp"), lax.axis_index("tp")
+    z, p = sp // plane, sp % plane
+    other = 1 - tp
+    tok = heads.shape[1]
+    half = tok // 2
+    val = heads.shape[2]
+    before = (p + plane - 1) % plane
+    peers = (
+        [(z * plane + (p + d) % plane, tp) for d in range(1, plane)]
+        + [((z + d) % planes * plane + p, tp) for d in range(1, planes)]
+        + [(sp, other)]
+    )
+    barrier = pltpu.get_barrier_semaphore()
+    for peer in peers + [(s * plane + before, 1) for s in range(planes)]:
+        pl.semaphore_signal(barrier, inc=1, device_id=peer, device_id_type=MESH)
+    pl.semaphore_wait(barrier, len(peers) + 2 * planes * tp)
+
+    started = []
+    own = pltpu.make_async_copy(head_out.at[block_of(p, tok), :], heads.at[p], own_sem)
+    own.start()
+    for d in range(1, plane):
+        there = (p + d) % plane
+        copy = remote(
+            head_out.at[block_of(there, tok), :], heads.at[p],
+            a_send.at[d], a_recv.at[d], z * plane + there, tp,
+        )
+        copy.start()
+        started.append(copy)
+    own.wait()
+    for d in range(1, plane):
+        there = (p + plane - d) % plane
+        remote(
+            heads.at[there], heads.at[there], a_send.at[d], a_recv.at[d], z * plane + there, tp
+        ).wait_recv()
+
+    columns = 512
+
+    def product(which, at):
+        total = None
+        for h in range(plane):
+            term = jnp.dot(
+                heads[h, block_of(which, half), :],
+                out_weight[h * val : (h + 1) * val, at : at + columns],
+                preferred_element_type=jnp.float32,
+            )
+            total = term if total is None else total + term
+        return total.astype(jnp.bfloat16)
+
+    model = out_weight.shape[1]
+    for at in range(0, model, columns):
+        part[:, at : at + columns] = product(other, at)
+    swap = remote(part, part_in, t_send, t_recv, sp, other)
+    swap.start()
+    started.append(swap)
+    for at in range(0, model, columns):
+        stream[:, at : at + columns] = product(tp, at).astype(jnp.float32)
+    swap.wait_recv()
+    whole = residual[...].astype(jnp.float32) + (stream[...] + part_in[...].astype(jnp.float32))
+    stream[...] = whole
+    scaled = whole * lax.rsqrt(jnp.mean(whole * whole, axis=-1, keepdims=True) + epsilon) * gain[...]
+    rounded = scaled.astype(jnp.bfloat16)
+    normed[z, block_of(tp, half), :] = rounded
+    tail[...] = scaled[half - 8 :, :].astype(jnp.bfloat16)
+
+    mine = normed.at[z, block_of(tp, half), :]
+    for d in range(1, planes):
+        copy = remote(mine, mine, z_send.at[d], z_recv.at[d], (z + d) % planes * plane + p, tp)
+        copy.start()
+        started.append(copy)
+    copy = remote(mine, mine, f_send.at[0], f_recv.at[0], sp, other)
+    copy.start()
+    started.append(copy)
+    after = (p + 1) % plane
+    zone = z + (p + 1) // plane
+
+    @pl.when(jnp.logical_and(tp == 1, zone < planes))
+    def _():
+        for s in range(planes):
+            for t in range(2):
+                remote(
+                    tail, halo.at[zone], h_send.at[s, t], h_recv.at[zone], s * plane + after, t
+                ).start()
+
+    for d in range(1, planes):
+        there = (z + planes - d) % planes
+        theirs = normed.at[there, block_of(tp, half), :]
+        remote(theirs, theirs, z_send.at[d], z_recv.at[d], sp, other).wait_recv()
+        copy = remote(theirs, theirs, f_send.at[d], f_recv.at[d], sp, other)
+        copy.start()
+        started.append(copy)
+    for d in range(planes):
+        theirs = normed.at[(z + planes - d) % planes, block_of(other, half), :]
+        remote(theirs, theirs, f_send.at[d], f_recv.at[d], sp, other).wait_recv()
+    for s in range(planes):
+
+        @pl.when(s * plane + p > 0)
+        def _():
+            remote(tail, halo.at[s], h_send.at[s, 0], h_recv.at[s], sp, other).wait_recv()
+
+        @pl.when(s * plane + p == 0)
+        def _():
+            halo[s] = jnp.zeros(halo.shape[1:], halo.dtype)
+
+    @pl.when(jnp.logical_and(tp == 1, zone < planes))
+    def _():
+        for s in range(planes):
+            for t in range(2):
+                remote(tail, halo.at[0], h_send.at[s, t], h_recv.at[0], sp, other).wait_send()
+
+    for copy in started:
+        copy.wait_send()
+
+
+def down_kernel(
+    plane, planes, starts, hidden, weight, stream, out,
+    units, total_buf, part, part_in, own_sem, a_send, a_recv, t_send, t_recv,
+):
+    sp, tp = lax.axis_index("sp"), lax.axis_index("tp")
+    z, p = sp // plane, sp % plane
+    other = 1 - tp
+    tok = units.shape[1]
+    half = tok // 2
+    greet([((z + d) % planes * plane + p, tp) for d in range(1, planes)] + [(sp, other)])
+    started = []
+    own = pltpu.make_async_copy(hidden.at[z], units.at[z], own_sem)
+    own.start()
+    for d in range(1, planes):
+        there = (z + d) % planes
+        copy = remote(
+            hidden.at[there], units.at[z], a_send.at[d], a_recv.at[d], there * plane + p, tp
+        )
+        copy.start()
+        started.append(copy)
+    own.wait()
+    for d in range(1, planes):
+        there = (z + planes - d) % planes
+        remote(
+            units.at[there], units.at[there], a_send.at[d], a_recv.at[d], sp, other
+        ).wait_recv()
+    model = weight.shape[1]
+    columns = 256
+
+    def product(which, at):
+        total = None
+        for s in range(planes):
+            term = jnp.dot(
+                units[s, block_of(which, half), 0 : starts[s + 1] - starts[s]],
+                weight[starts[s] : starts[s + 1], block_of(at, columns)],
+                preferred_element_type=jnp.float32,
+            )
+            total = term if total is None else total + term
+        return total.astype(jnp.bfloat16)
+
+    @pl.loop(0, model // columns)
+    def _(at):
+        part[:, block_of(at, columns)] = product(other, at)
+
+    swap = remote(part, part_in, t_send, t_recv, sp, other)
+    swap.start()
+    started.append(swap)
+
+    @pl.loop(0, model // columns)
+    def _(at):
+        here = block_of(at, columns)
+        total_buf[:, here] = stream[:, here] + product(tp, at).astype(jnp.float32)
+
+    swap.wait_recv()
+    out[...] = (total_buf[...] + part_in[...].astype(jnp.float32)).astype(out.dtype)
+    for copy in started:
+        copy.wait_send()
+
+
+def shorter_routes(
+    plane, planes,
+    query_one, key_one, query_two, key_two, values, mix_weight, head_gain, residual, out_weight,
+    norm_gain, lift_weight, gate_weight, conv_taps, down_weight,
+):
+    bf16, f32 = jnp.bfloat16, jnp.float32
+    tok = query_one.shape[0]
+    model = residual.shape[1]
+    val = 2 * HD
+    ff = lift_weight.shape[1]
+    tiles = ff // 128
+    starts = [s * tiles // planes * 128 for s in range(planes + 1)]
+    width = -(-tiles // planes) * 128
+    count = planes * plane * tok
+    sp = lax.axis_index("sp")
+    z, p = sp // plane, sp % plane
+    dma = pltpu.SemaphoreType.DMA
+    anywhere = pl.BlockSpec(memory_space=pl.ANY)
+    local = pl.BlockSpec(memory_space=pltpu.VMEM)
+    shape = jax.ShapeDtypeStruct
+
+    q_all, kv_all, lift_all, gate_all = pl.pallas_call(
+        functools.partial(spread_kernel, plane, planes, width),
+        out_shape=(
+            shape((plane * tok, 2 * HD), bf16),
+            shape((count, 4 * HD), bf16),
+            shape((count, width), bf16),
+            shape((count, width), bf16),
+        ),
+        in_specs=[anywhere] * 7,
+        out_specs=(anywhere,) * 4,
+        scratch_shapes=[
+            dma((7,)), dma((plane, 5)), dma((plane, 5)), dma((planes, 2)), dma((planes, 2)),
+            dma((planes,)), dma((planes,)), dma((planes, plane, 2)), dma((planes, plane, 2)),
+        ],
+        compiler_params=pltpu.CompilerParams(collective_id=0, has_side_effects=True),
+        name="spread",
+    )(query_one, key_one, query_two, key_two, values, lift_weight, gate_weight)
+
+    k_pos = lax.iota(jnp.int32, count)
+    q_pos = z * plane * tok + lax.iota(jnp.int32, plane * tok)
+    visible = k_pos[None, :] // STRETCH <= q_pos[:, None] // STRETCH
+    arrived = k_pos[:, None] < (z + 1) * plane * tok
+    vals = jnp.where(arrived, kv_all[:, 2 * HD :], 0)
+
+    def one_map(index):
+        queries = q_all[:, index * HD : (index + 1) * HD]
+        keys = kv_all[:, index * HD : (index + 1) * HD]
+        scores = jnp.einsum("td,sd->ts", queries, keys, preferred_element_type=f32) * HD**-0.5
+        scores = jnp.where(visible, scores, masked_score)
+        weights = jnp.where(visible, jnp.exp(scores - jnp.max(scores, axis=-1, keepdims=True)), 0.0)
+        total = jnp.sum(weights, axis=-1, keepdims=True)
+        return jnp.dot(weights.astype(bf16), vals, preferred_element_type=f32) / total
+
+    mixed = one_map(0) - mix_weight[p] * one_map(1)
+    head_out = (
+        mixed * lax.rsqrt(jnp.mean(mixed * mixed, axis=-1, keepdims=True) + epsilon) * head_gain
+    ).astype(bf16)
+
+    normed, halo, stream = pl.pallas_call(
+        functools.partial(out_kernel, plane, planes),
+        out_shape=(
+            shape((planes, tok, model), bf16),
+            shape((planes, 8, model), bf16),
+            shape((tok // 2, model), f32),
+        ),
+        in_specs=[local] * 4,
+        out_specs=(local,) * 3,
+        scratch_shapes=[
+            pltpu.VMEM((plane, tok, val), bf16),
+            pltpu.VMEM((tok // 2, model), bf16),
+            pltpu.VMEM((tok // 2, model), bf16),
+            pltpu.VMEM((8, model), bf16),
+            dma, dma((plane,)), dma((plane,)), dma, dma,
+            dma((planes,)), dma((planes,)), dma((planes,)), dma((planes,)),
+            dma((planes, 2)), dma((planes,)),
+        ],
+        compiler_params=pltpu.CompilerParams(
+            collective_id=1, has_side_effects=True, vmem_limit_bytes=32 << 20
+        ),
+        name="project",
+    )(head_out, out_weight, residual, norm_gain.reshape(1, model))
+
+    rows = jnp.concatenate([halo, normed], axis=1).reshape(planes * (tok + 8), model)
+    lifted = jnp.dot(rows, lift_all, preferred_element_type=f32).astype(bf16)
+    gated = jnp.dot(rows, gate_all, preferred_element_type=f32).astype(bf16)
+    lifted = lifted.reshape(planes, tok + 8, width)[:, 8:].astype(f32)
+    gated = gated.reshape(planes, tok + 8, width).astype(f32)
+    taps = lax.dynamic_slice_in_dim(conv_taps, z * tiles // planes * 128, width, 1)
+    conv = 0.0
+    for index in range(WIDTH):
+        at = 8 - (WIDTH - 1) + index
+        conv = conv + taps[index] * gated[:, at : at + tok]
+    hidden = (jax.nn.silu(conv) * lifted).astype(bf16)
+
+    return pl.pallas_call(
+        functools.partial(down_kernel, plane, planes, starts),
+        out_shape=shape((tok // 2, model), bf16),
+        in_specs=[local] * 3,
+        out_specs=local,
+        scratch_shapes=[
+            pltpu.VMEM((planes, tok, width), bf16),
+            pltpu.VMEM((tok // 2, model), f32),
+            pltpu.VMEM((tok // 2, model), bf16),
+            pltpu.VMEM((tok // 2, model), bf16),
+            dma, dma((planes,)), dma((planes,)), dma, dma,
+        ],
+        compiler_params=pltpu.CompilerParams(
+            collective_id=2, has_side_effects=True, vmem_limit_bytes=40 << 20
+        ),
+        name="down",
+    )(hidden, down_weight, stream)
+
+
+def any_route(*arrays):
+    tok, heads, ff = arrays[0].shape[0], arrays[5].shape[0], arrays[10].shape[1]
+    devices, groups = lax.axis_size("sp"), lax.axis_size("tp")
+    planes = devices // heads
+    fits = (
+        groups == 2 and heads > 1 and planes > 1 and devices % heads == 0
+        and ff % 128 == 0 and tok % 128 == 0 and WIDTH <= 9
+        and arrays[10].shape[0] == tok
+    )
+    if fits:
+        return shorter_routes(heads, planes, *arrays)
+    return on_device(*arrays)
+
 
 def solution(mesh):
     return jax.shard_map(
-        on_device,
+        any_route,
         mesh=mesh,
         in_specs=(
             P("sp", "tp"),

time: 560 us -> 175 us (0.31)
  waiting for transfers between devices: 489 us -> 0 us
  Pallas kernels: 0 us -> 148 us
  matrix products: 37 us -> 14 us
  between operations: 13.6 us -> 0.28 us
    all_gather x5 -> x0, waiting for transfers between devices: 469 us -> none  [the longest x1 138 us: on_device(): lax.all_gather(gate_weight, 'sp', axis=0, tiled=True)]
    pallas_call x0 -> x3, Pallas kernels: none -> 148 us  [the longest x1 82.9 us: shorter_routes(): pl.pallas_call(functools.partial(spread_kernel, plane, planes, width), ou...]
    dot_general x7 -> x6, matrix products: 37 us -> 14 us  [the longest x2 5.85 us: one_map(): jnp.dot(weights.astype(bf16), vals, preferred_element_type=f32) / total]
    reduce_scatter x2 -> x0, waiting for transfers between devices: 16.4 us -> none  [the longest x1 8.81 us: on_device(): lax.psum_scatter(jnp.dot(piece, down_weight, preferred_element_type=jnp.f...]
  transfers between devices with their start and end apart: 8 -> 0, of which waited for: 8 -> 0; matrix products, arithmetic and copies ran while one was open for 4% -> 0% of each run, Pallas kernels for 0% -> 0%
where the time goes in v1:
time: 175 us; the launch traced here: 174 us
  Pallas kernels  148 us (85%)
  matrix products  14 us (8%)
  local copies, waits for them, and re-layouts  9.1 us (5%)
  other arithmetic  2.54 us (1%)
    pallas_call x1, Pallas kernels, shorter_routes(): pl.pallas_call(functools.partial(spread_kernel, plane, planes, width), ou...  82.9 us
    pallas_call x1, Pallas kernels, shorter_routes(): pl.pallas_call(functools.partial(out_kernel, plane, planes), out_shape=(s...  39.5 us
    pallas_call x1, Pallas kernels, shorter_routes(): pl.pallas_call(functools.partial(down_kernel, plane, planes, starts), out...  26.1 us
    unnamed x27, local copies, waits for them, and re-layouts  7.6 us
    dot_general x2, matrix products, one_map(): jnp.dot(weights.astype(bf16), vals, preferred_element_type=f32) / total  5.85 us
    dot_general x2, matrix products, one_map(): jnp.einsum('td,sd->ts', queries, keys, preferred_element_type=f32)  4.33 us

profile of v1, /device:TPU:25, one launch (start us, length us, event | category | flops | bytes accessed | tf_op | source)
XLA Modules:
  0.0 174.4 jit_solution(13497611661714285677)
XLA Ops:
  0.0 82.9 %spread.1 = (bf16[512,256]{1,0:T(8,128)(2,1)}, bf16[2048,512]{1,0:T(8,128)(2,1)}, bf16[2048,768]{1,0:T(8,128)(2,1)}, bf16[2048,768]{1,0:T(8,128)(2,1)}) custom-call(bf16[128,512]{1,0:T(8,128)(2,1)} %q1.1, bf16[128,512]{1,0:T(8,128)(2,1)} %k1.1, bf16[128,512]{1,0:T(8,128)(2,1)} %q2.1, bf16[128,512]{1,0:T(8,128)(2,1)} %k2.1, bf16[128,1024]{1,0:T(8,128)(2,1)} %v.1, ...), custom_call_target="tpu_custom_call" | custom-call | tf_op jit(solution)/shard_map/spread/pallas_call | solution.py:461
  82.9 0.0 copy-start.8
  82.9 0.0 copy-start.9
  82.9 2.2 %fusion = (f32[512]{0:T(512)S(1)}, f32[512,2048]{1,0:T(8,128)S(1)}) fusion(s32[2048]{0:T(1024)S(1)} %add_select_fusion, s32[512]{0:T(512)S(1)} %add_select_fusion.1, bf16[2048,512]{1,0:T(8,128)(2,1)} %get-tuple-element.13, bf16[512,256]{1,0:T(8,128)(2,1)} %get-tuple-element.12), kind=kOutput, calls=%fused_computation.4 | convolution fusion | flops 272629248 | bytes 4861952 | tf_op jit(solution)/shard_map/td,sd->ts/dot_general | solution.py:488
  85.1 0.0 copy-done.8
  85.1 0.0 copy-done.9
  85.1 2.1 %fusion.2 = (f32[512]{0:T(512)S(1)}, f32[512]{0:T(512)S(1)}, f32[512,2048]{1,0:T(8,128)S(1)}) fusion(f32[512,2048]{1,0:T(8,128)S(1)} %get-tuple-element.25, f32[512]{0:T(512)S(1)} %get-tuple-element.24, s32[2048]{0:T(1024)S(1)} %add_select_fusion, s32[512]{0:T(512)S(1)} %add_select_fusion.1, bf16[2048,512]{1,0:T(8,128)(2,1)S(1)} %copy-done.8, ...), kind=kOutput, calls=%fused_computation.6 | convolution fusion | flops 277871616 | bytes 9060352 | tf_op jit(solution)/shard_map/td,sd->ts/dot_general | solution.py:488
  87.3 0.0 copy-done.11
  87.3 0.0 copy-start.10
  87.3 2.0 %copy-done.4 = f32[512,2048]{1,0:T(8,128)} copy-done((f32[512,2048]{1,0:T(8,128)}, f32[512,2048]{1,0:T(8,128)S(1)}, u32[]{:S(2)}) %copy-start.4) | copy-done | bytes 4194328
  89.2 1.2 fusion.4
  90.5 0.6 dynamic_slice.7
  91.1 4.4 %fusion.21 = f32[512,256]{1,0:T(8,128)S(1)} fusion(f32[512,2048]{1,0:T(8,128)} %copy-done.4, f32[512]{0:T(512)S(1)} %get-tuple-element.23, s32[2048]{0:T(1024)S(1)} %add_select_fusion, s32[512]{0:T(512)S(1)} %add_select_fusion.1, bf16[2048,512]{1,0:T(8,128)(2,1)S(1)} %copy-done.8, pred[2048]{0:T(1024)(128)(4,1)S(1)} %iota_compare_fusion, ...), kind=kOutput, calls=%fused_computation.25 | convolution fusion | flops 543948800 | bytes 5783556 | tf_op jit(solution)/shard_map/dot_general | solution.py:492
  95.6 0.0 copy-start.5
  95.6 0.0 copy-start.1
  95.6 0.0 copy-start.2
  95.6 0.0 copy-start.3
  95.6 1.4 multiply_reduce_fusion
  97.0 0.1 multiply_convert_fusion.1.head_out
  97.2 0.6 copy-done.1
  97.8 0.0 copy-done.2
  97.8 39.5 %project.1 = (bf16[4,128,2048]{2,1,0:T(8,128)(2,1)S(1)}, bf16[4,8,2048]{2,1,0:T(8,128)(2,1)S(1)}, f32[64,2048]{1,0:T(8,128)S(1)}) custom-call(bf16[512,256]{1,0:T(8,128)(2,1)S(1)} %multiply_convert_fusion.1.head_out, bf16[1024,2048]{1,0:T(8,128)(2,1)S(1)} %copy-done.1, bf16[64,2048]{1,0:T(8,128)(2,1)S(1)} %copy-done.2, f32[1,2048]{1,0:T(1,128)S(1)} %bitcast.10), custom_call_target="tpu_custom_call" | custom-call | tf_op jit(solution)/shard_map/project/pallas_call | solution.py:499
  137.3 0.1 pad_maximum_fusion
  137.5 1.9 %convolution_convert_fusion = bf16[544,768]{1,0:T(8,128)(2,1)S(1)} fusion(bf16[544,2048]{1,0:T(8,128)(2,1)S(1)} %bitcast.11, bf16[2048,768]{1,0:T(8,128)(2,1)S(1)} %copy-done.7), kind=kOutput, calls=%fused_computation.19 | convolution fusion | flops 1711693824 | bytes 6209536 | tf_op jit(solution)/shard_map/dot_general | solution.py:524
  139.4 1.9 %convolution_convert_fusion.1 = bf16[544,768]{1,0:T(8,128)(2,1)S(1)} fusion(bf16[544,2048]{1,0:T(8,128)(2,1)S(1)} %bitcast.12, bf16[2048,768]{1,0:T(8,128)(2,1)S(1)} %copy-done.6), kind=kOutput, calls=%fused_computation.20 | convolution fusion | flops 1711693824 | bytes 6209536 | tf_op jit(solution)/shard_map/dot_general | solution.py:525
  141.3 0.1 convert.1
  141.5 0.9 dynamic-slice_reduce_fusion.2
  142.4 0.9 multiply_convert_fusion.hidden
  143.3 0.0 copy-start
  143.3 4.3 %copy-done = bf16[2816,2048]{1,0:T(8,128)(2,1)S(1)} copy-done((bf16[2816,2048]{1,0:T(8,128)(2,1)S(1)}, bf16[2816,2048]{1,0:T(8,128)(2,1)}, u32[]{:S(2)}) %copy-start) | copy-done | bytes 11534360
  147.6 26.1 %down.1 = bf16[64,2048]{1,0:T(8,128)(2,1)S(1)} custom-call(bf16[4,128,768]{2,1,0:T(8,128)(2,1)S(1)} %multiply_convert_fusion.hidden, bf16[2816,2048]{1,0:T(8,128)(2,1)S(1)} %copy-done, f32[64,2048]{1,0:T(8,128)S(1)} %get-tuple-element.18.stream), custom_call_target="tpu_custom_call" | custom-call | tf_op jit(solution)/shard_map/down/pallas_call | solution.py:535
  173.6 0.7 copy.20
  (15 shorter events, 0.1 us)
Async XLA Ops:
  82.9 2.2 %copy-start.8 = (bf16[2048,512]{1,0:T(8,128)(2,1)S(1)}, bf16[2048,512]{1,0:T(8,128)(2,1)}, u32[]{:S(2)}) copy-start(bf16[2048,512]{1,0:T(8,128)(2,1)} %get-tuple-element.13) | copy-start | bytes 6291460
  82.9 2.2 %copy-start.9 = (bf16[512,256]{1,0:T(8,128)(2,1)S(1)}, bf16[512,256]{1,0:T(8,128)(2,1)}, u32[]{:S(2)}) copy-start(bf16[512,256]{1,0:T(8,128)(2,1)} %get-tuple-element.12) | copy-start | bytes 786436
  85.1 2.2 %copy-start.11 = (f32[512,2048]{1,0:T(8,128)}, f32[512,2048]{1,0:T(8,128)S(1)}, u32[]{:S(2)}) copy-start(f32[512,2048]{1,0:T(8,128)S(1)} %get-tuple-element.25) | copy-start | bytes 12582916
  87.3 2.0 %copy-start.4 = (f32[512,2048]{1,0:T(8,128)}, f32[512,2048]{1,0:T(8,128)S(1)}, u32[]{:S(2)}) copy-start(f32[512,2048]{1,0:T(8,128)S(1)} %get-tuple-element.26) | copy-start | bytes 12582916
  87.3 3.2 %copy-start.10 = (f32[4]{0:T(128)S(1)}, f32[4]{0:T(128)}, u32[]{:S(2)}) copy-start(f32[4]{0:T(128)} %param.19) | copy-start | bytes 52
  91.1 4.5 %copy-start.12 = (f32[512,2048]{1,0:T(8,128)S(1)}, f32[512,2048]{1,0:T(8,128)}, u32[]{:S(2)}) copy-start(f32[512,2048]{1,0:T(8,128)} %copy-done.11) | copy-start | bytes 12582916
  95.6 1.5 copy-start.5
  95.6 2.2 %copy-start.1 = (bf16[1024,2048]{1,0:T(8,128)(2,1)S(1)}, bf16[1024,2048]{1,0:T(8,128)(2,1)}, u32[]{:S(2)}) copy-start(bf16[1024,2048]{1,0:T(8,128)(2,1)} %out_weight.1) | copy-start | bytes 12582916
  95.6 2.2 %copy-start.2 = (bf16[64,2048]{1,0:T(8,128)(2,1)S(1)}, bf16[64,2048]{1,0:T(8,128)(2,1)}, u32[]{:S(2)}) copy-start(bf16[64,2048]{1,0:T(8,128)(2,1)} %residual.1) | copy-start | bytes 786436
  95.6 2.2 %copy-start.3 = (f32[2048]{0:T(1024)S(1)}, f32[2048]{0:T(1024)}, u32[]{:S(2)}) copy-start(f32[2048]{0:T(1024)} %param.23) | copy-start | bytes 24580
  97.8 39.7 %copy-start.7 = (bf16[2048,768]{1,0:T(8,128)(2,1)S(1)}, bf16[2048,768]{1,0:T(8,128)(2,1)}, u32[]{:S(2)}) copy-start(bf16[2048,768]{1,0:T(8,128)(2,1)} %get-tuple-element.17) | copy-start | bytes 9437188
  137.5 1.9 %copy-start.6 = (bf16[2048,768]{1,0:T(8,128)(2,1)S(1)}, bf16[2048,768]{1,0:T(8,128)(2,1)}, u32[]{:S(2)}) copy-start(bf16[2048,768]{1,0:T(8,128)(2,1)} %get-tuple-element.16) | copy-start | bytes 9437188
  143.3 4.3 %copy-start = (bf16[2816,2048]{1,0:T(8,128)(2,1)S(1)}, bf16[2816,2048]{1,0:T(8,128)(2,1)}, u32[]{:S(2)}) copy-start(bf16[2816,2048]{1,0:T(8,128)(2,1)} %weight.1) | copy-start | bytes 34603012

commit v2 on v1

--- a/solution.py
+++ b/solution.py
@@ -149,147 +149,191 @@
     return pl.ds(pl.multiple_of(index * size, size), size)
 
 
-def spread_kernel(
-    plane, planes, width, q1, k1, q2, k2, v, lift, gate,
-    q_all, kv_all, lift_all, gate_all,
+def front_kernel(
+    plane, planes, width, q1, k1, q2, k2, v, lift, gate, mix_weight, head_gain, out_weight, residual,
+    gain,
+    lift_all, gate_all, normed, halo, stream,
+    q_all, kv_all, peaks, totals, sums, head_out, heads, part, part_in, tail,
     own_sem, a_send, a_recv, w_send, w_recv, kv_send, kv_recv, g_send, g_recv,
+    b_own, b_send, b_recv, t_send, t_recv, up_send, up_recv, down_send, down_recv,
+    f_send, f_recv, h_send, h_recv,
 ):
     sp, tp = lax.axis_index("sp"), lax.axis_index("tp")
     z, p = sp // plane, sp % plane
+    other = 1 - tp
     tok = q1.shape[0]
+    half = tok // 2
+    val = 2 * HD
     tiles = lift.shape[1] // 128
-    greet(
+    before = (p + plane - 1) % plane
+    above, below = (z + 1) % planes * plane + p, (z + planes - 1) % planes * plane + p
+    weights = ((lift, lift_all), (gate, gate_all))
+    peers = (
         [(z * plane + (p + d) % plane, tp) for d in range(1, plane)]
         + [((z + d) % planes * plane + p, tp) for d in range(1, planes)]
-    )
+        + [(sp, other)]
+    )
+    barrier = pltpu.get_barrier_semaphore()
+    for peer in peers + [(s * plane + before, 1) for s in range(planes)]:
+        pl.semaphore_signal(barrier, inc=1, device_id=peer, device_id_type=MESH)
 
     def piece(head, row):
         h1, h2 = block_of(head, HD), block_of(head, 2 * HD)
         rows, all_rows = block_of(row % plane, tok), block_of(row, tok)
         return [
-            (q1.at[:, h1], q_all.at[rows, 0:HD]),
-            (q2.at[:, h1], q_all.at[rows, HD : 2 * HD]),
             (k1.at[:, h1], kv_all.at[all_rows, 0:HD]),
             (k2.at[:, h1], kv_all.at[all_rows, HD : 2 * HD]),
             (v.at[:, h2], kv_all.at[all_rows, 2 * HD : 4 * HD]),
+            (q1.at[:, h1], q_all.at[rows, 0:HD]),
+            (q2.at[:, h1], q_all.at[rows, HD : 2 * HD]),
         ]
 
     def units(index):
         return pl.ds(pl.multiple_of(index * tiles // planes * 128, 128), width)
 
     started = []
-    own = []
-    for n, (src, dst) in enumerate(piece(p, sp)):
-        own.append(pltpu.make_async_copy(src, dst, own_sem.at[n]))
-    for m, (src, dst) in enumerate(((lift, lift_all), (gate, gate_all))):
-        own.append(
-            pltpu.make_async_copy(src.at[:, units(z)], dst.at[block_of(sp, tok), :], own_sem.at[5 + m])
-        )
+    own = [
+        pltpu.make_async_copy(src, dst, own_sem.at[n]) for n, (src, dst) in enumerate(piece(p, sp))
+    ]
+    own_weights = [
+        pltpu.make_async_copy(src.at[:, units(z)], dst.at[block_of(sp, tok), :], own_sem.at[5 + m])
+        for m, (src, dst) in enumerate(weights)
+    ]
     for copy in own:
         copy.start()
+    pl.semaphore_wait(barrier, len(peers) + 2 * planes * tp)
     for d in range(1, plane):
         there = (p + d) % plane
         for n, (src, dst) in enumerate(piece(there, sp)):
             copy = remote(src, dst, a_send.at[d, n], a_recv.at[d, n], z * plane + there, tp)
             copy.start()
             started.append(copy)
-    for d in range(1, planes):
+
+    def send_weights(d):
         there = (z + d) % planes
-        for m, (src, dst) in enumerate(((lift, lift_all), (gate, gate_all))):
+        for m, (src, dst) in enumerate(weights):
             copy = remote(
                 src.at[:, units(there)], dst.at[block_of(sp, tok), :],
                 w_send.at[d, m], w_recv.at[d, m], there * plane + p, tp,
             )
             copy.start()
             started.append(copy)
-    for m, (src, dst) in enumerate(((lift, lift_all), (gate, gate_all))):
-        for e in range(1, plane):
-            copy = remote(
-                src.at[:, units(z)], dst.at[block_of(sp, tok), :],
-                g_send.at[0, e, m], g_recv.at[0, e, m], z * plane + (p + e) % plane, tp,
-            )
-            copy.start()
-            started.append(copy)
+
+    def share_weights(d):
+        source = (z + planes - d) % planes * plane + p
+        rows = block_of(source, tok)
+        for m, dst in enumerate((lift_all, gate_all)):
+            if d:
+                remote(
+                    dst.at[rows, :], dst.at[rows, :], w_send.at[d, m], w_recv.at[d, m], source, tp
+                ).wait_recv()
+            src = dst.at[rows, :] if d else weights[m][0].at[:, units(z)]
+            for e in range(1, plane):
+                copy = remote(
+                    src, dst.at[rows, :], g_send.at[d, e, m], g_recv.at[d, e, m],
+                    z * plane + (p + e) % plane, tp,
+                )
+                copy.start()
+                started.append(copy)
+
+    if planes > 2:
+        send_weights(planes - 1)
+    share_weights(0)
+    for copy in own_weights:
+        copy.start()
     for copy in own:
         copy.wait()
     for d in range(1, plane):
         source = z * plane + (p + plane - d) % plane
         for n, (src, dst) in enumerate(piece(p, source)):
             remote(src, dst, a_send.at[d, n], a_recv.at[d, n], source, tp).wait_recv()
-    mine = kv_all.at[block_of(z, plane * tok), :]
+
+    span = plane * tok
+
+    def keys_of(index):
+        return kv_all.at[block_of(index, span), :]
+
+    @pl.when(z + 1 < planes)
+    def _():
+        remote(keys_of(z), keys_of(z), kv_send.at[1], kv_recv.at[1], above, tp).start()
+
+    def attend(source, first):
+        @pl.loop(0, plane)
+        def _(chunk):
+            rows, keys = block_of(chunk, tok), block_of(source, span)
+            for m in range(2):
+                scores = lax.dot_general(
+                    q_all[rows, m * HD : (m + 1) * HD],
+                    kv_all[keys, m * HD : (m + 1) * HD],
+                    (((1,), (1,)), ((), ())),
+                    preferred_element_type=jnp.float32,
+                ) * HD ** (-0.5)
+                if first:
+                    k_pos = lax.broadcasted_iota(jnp.int32, (tok, span), 1)
+                    q_pos = chunk * tok + lax.broadcasted_iota(jnp.int32, (tok, span), 0)
+                    visible = lax.div(k_pos, STRETCH) <= lax.div(q_pos, STRETCH)
+                    scores = jnp.where(visible, scores, masked_score)
+                    peak = jnp.max(scores, axis=-1, keepdims=True)
+                    terms = jnp.where(visible, jnp.exp(scores - peak), 0.0)
+                else:
+                    last = peaks[m, rows, 0:1]
+                    peak = jnp.maximum(last, jnp.max(scores, axis=-1, keepdims=True))
+                    terms = jnp.exp(scores - peak)
+                total = jnp.sum(terms, axis=-1, keepdims=True)
+                acc = jnp.dot(
+                    terms.astype(jnp.bfloat16),
+                    kv_all[keys, 2 * HD : 4 * HD],
+                    preferred_element_type=jnp.float32,
+                )
+                if not first:
+                    fade = jnp.exp(last - peak)
+                    total = total + fade * totals[m, rows, 0:1]
+                    acc = acc + fade * sums[m, rows, :]
+                peaks[m, rows, :] = jnp.broadcast_to(peak, (tok, HD))
+                totals[m, rows, :] = jnp.broadcast_to(total, (tok, HD))
+                sums[m, rows, :] = acc
+
+    attend(z, True)
     for d in range(1, planes):
-
-        @pl.when(z + d < planes)
-        def _():
-            remote(mine, mine, kv_send.at[d], kv_recv.at[d], (z + d) % planes * plane + p, tp).start()
-
-    for d in range(1, planes):
-        source = (z + planes - d) % planes * plane + p
-        rows = block_of(source, tok)
-        for m, dst in enumerate((lift_all, gate_all)):
-            remote(dst.at[rows, :], dst.at[rows, :], w_send.at[d, m], w_recv.at[d, m], source, tp).wait_recv()
-            for e in range(1, plane):
-                copy = remote(
-                    dst.at[rows, :], dst.at[rows, :],
-                    g_send.at[d, e, m], g_recv.at[d, e, m], z * plane + (p + e) % plane, tp,
-                )
-                copy.start()
-                started.append(copy)
-    for d in range(planes):
-        for e in range(1, plane):
-            there = (p + plane - e) % plane
-            rows = block_of((z + planes - d) % planes * plane + there, tok)
-            for m, dst in enumerate((lift_all, gate_all)):
-                remote(
-                    dst.at[rows, :], dst.at[rows, :], g_send.at[d, e, m], g_recv.at[d, e, m],
-                    z * plane + there, tp,
-                ).wait_recv()
-    for d in range(1, planes):
-        below = kv_all.at[block_of((z + planes - d) % planes, plane * tok), :]
+        here = keys_of((z + planes - d) % planes)
 
         @pl.when(z - d >= 0)
         def _():
-            remote(below, below, kv_send.at[d], kv_recv.at[d], sp, tp).wait_recv()
-
-        @pl.when(z + d < planes)
-        def _():
-            remote(mine, mine, kv_send.at[d], kv_recv.at[d], sp, tp).wait_send()
-
-    for copy in started:
-        copy.wait_send()
-
-
-def out_kernel(
-    plane, planes, head_out, out_weight, residual, gain,
-    normed, halo, stream,
-    heads, part, part_in, tail, own_sem, a_send, a_recv, t_send, t_recv,
-    z_send, z_recv, f_send, f_recv, h_send, h_recv,
-):
-    sp, tp = lax.axis_index("sp"), lax.axis_index("tp")
-    z, p = sp // plane, sp % plane
-    other = 1 - tp
-    tok = heads.shape[1]
-    half = tok // 2
-    val = heads.shape[2]
-    before = (p + plane - 1) % plane
-    peers = (
-        [(z * plane + (p + d) % plane, tp) for d in range(1, plane)]
-        + [((z + d) % planes * plane + p, tp) for d in range(1, planes)]
-        + [(sp, other)]
-    )
-    barrier = pltpu.get_barrier_semaphore()
-    for peer in peers + [(s * plane + before, 1) for s in range(planes)]:
-        pl.semaphore_signal(barrier, inc=1, device_id=peer, device_id_type=MESH)
-    pl.semaphore_wait(barrier, len(peers) + 2 * planes * tp)
-
-    started = []
-    own = pltpu.make_async_copy(head_out.at[block_of(p, tok), :], heads.at[p], own_sem)
+            remote(here, here, kv_send.at[d], kv_recv.at[d], below, tp).wait_recv()
+
+            @pl.when(z + 1 < planes)
+            def _():
+                remote(here, here, kv_send.at[d + 1], kv_recv.at[d + 1], above, tp).start()
+
+        if d < planes - 1:
+            send_weights(planes - 1 - d)
+        elif planes == 2:
+            send_weights(1)
+
+        @pl.when(z - d >= 0)
+        def _():
+            attend((z + planes - d) % planes, False)
+
+        if d == 1 and planes > 2:
+            share_weights(planes - 1)
+
+    @pl.loop(0, plane)
+    def _(chunk):
+        rows = block_of(chunk, tok)
+        mixed = (
+            sums[0, rows, :] / totals[0, rows, 0:1]
+            - mix_weight[p] * sums[1, rows, :] / totals[1, rows, 0:1]
+        )
+        scale = lax.rsqrt(jnp.mean(mixed * mixed, axis=-1, keepdims=True) + epsilon)
+        head_out[rows, :] = (mixed * scale * head_gain[...]).astype(jnp.bfloat16)
+
+    own = pltpu.make_async_copy(head_out.at[block_of(p, tok), :], heads.at[p], b_own)
     own.start()
     for d in range(1, plane):
         there = (p + d) % plane
         copy = remote(
             head_out.at[block_of(there, tok), :], heads.at[p],
-            a_send.at[d], a_recv.at[d], z * plane + there, tp,
+            b_send.at[d], b_recv.at[d], z * plane + there, tp,
         )
         copy.start()
         started.append(copy)
@@ -297,7 +341,7 @@
     for d in range(1, plane):
         there = (p + plane - d) % plane
         remote(
-            heads.at[there], heads.at[there], a_send.at[d], a_recv.at[d], z * plane + there, tp
+            heads.at[there], heads.at[there], b_send.at[d], b_recv.at[d], z * plane + there, tp
         ).wait_recv()
 
     columns = 512
@@ -325,18 +369,23 @@
     whole = residual[...].astype(jnp.float32) + (stream[...] + part_in[...].astype(jnp.float32))
     stream[...] = whole
     scaled = whole * lax.rsqrt(jnp.mean(whole * whole, axis=-1, keepdims=True) + epsilon) * gain[...]
-    rounded = scaled.astype(jnp.bfloat16)
-    normed[z, block_of(tp, half), :] = rounded
+    normed[z, block_of(tp, half), :] = scaled.astype(jnp.bfloat16)
     tail[...] = scaled[half - 8 :, :].astype(jnp.bfloat16)
 
-    mine = normed.at[z, block_of(tp, half), :]
-    for d in range(1, planes):
-        copy = remote(mine, mine, z_send.at[d], z_recv.at[d], (z + d) % planes * plane + p, tp)
-        copy.start()
-        started.append(copy)
-    copy = remote(mine, mine, f_send.at[0], f_recv.at[0], sp, other)
-    copy.start()
-    started.append(copy)
+    def tokens(index, which):
+        return normed.at[index % planes, block_of(which, half), :]
+
+    mine = tokens(z, tp)
+
+    @pl.when(z + 1 < planes)
+    def _():
+        remote(mine, mine, up_send.at[1], up_recv.at[1], above, tp).start()
+
+    @pl.when(z > 0)
+    def _():
+        remote(mine, mine, down_send.at[1], down_recv.at[1], below, tp).start()
+
+    remote(mine, mine, f_send.at[0], f_recv.at[0], sp, other).start()
     after = (p + 1) % plane
     zone = z + (p + 1) // plane
 
@@ -349,15 +398,38 @@
                 ).start()
 
     for d in range(1, planes):
-        there = (z + planes - d) % planes
-        theirs = normed.at[there, block_of(tp, half), :]
-        remote(theirs, theirs, z_send.at[d], z_recv.at[d], sp, other).wait_recv()
-        copy = remote(theirs, theirs, f_send.at[d], f_recv.at[d], sp, other)
-        copy.start()
-        started.append(copy)
+
+        @pl.when(z - d >= 0)
+        def _():
+            theirs = tokens(z + planes - d, tp)
+            remote(theirs, theirs, up_send.at[d], up_recv.at[d], below, tp).wait_recv()
+
+            @pl.when(z + 1 < planes)
+            def _():
+                remote(theirs, theirs, up_send.at[d + 1], up_recv.at[d + 1], above, tp).start()
+
+            remote(theirs, theirs, f_send.at[d], f_recv.at[d], sp, other).start()
+
+        @pl.when(z + d < planes)
+        def _():
+            theirs = tokens(z + d, tp)
+            remote(theirs, theirs, down_send.at[d], down_recv.at[d], above, tp).wait_recv()
+
+            @pl.when(z > 0)
+            def _():
+                remote(theirs, theirs, down_send.at[d + 1], down_recv.at[d + 1], below, tp).start()
+
+            at = planes - d
+            remote(theirs, theirs, f_send.at[at], f_recv.at[at], sp, other).start()
+
+        if d < planes - 1:
+            share_weights(planes - 1 - d)
+        elif planes == 2:
+            share_weights(1)
+
     for d in range(planes):
-        theirs = normed.at[(z + planes - d) % planes, block_of(other, half), :]
-        remote(theirs, theirs, f_send.at[d], f_recv.at[d], sp, other).wait_recv()
+        theirs = tokens(z + planes - d, other)
+        remote(theirs, theirs, f_send.at[d], f_recv.at[d], sp, other).wait()
     for s in range(planes):
 
         @pl.when(s * plane + p > 0)
@@ -367,12 +439,35 @@
         @pl.when(s * plane + p == 0)
         def _():
             halo[s] = jnp.zeros(halo.shape[1:], halo.dtype)
+
+    for copy in own_weights:
+        copy.wait()
+    for d in range(planes):
+        for e in range(1, plane):
+            there = (p + plane - e) % plane
+            rows = block_of((z + planes - d) % planes * plane + there, tok)
+            for m, dst in enumerate((lift_all, gate_all)):
+                remote(
+                    dst.at[rows, :], dst.at[rows, :], g_send.at[d, e, m], g_recv.at[d, e, m],
+                    z * plane + there, tp,
+                ).wait_recv()
 
     @pl.when(jnp.logical_and(tp == 1, zone < planes))
     def _():
         for s in range(planes):
             for t in range(2):
                 remote(tail, halo.at[0], h_send.at[s, t], h_recv.at[0], sp, other).wait_send()
+
+    for d in range(1, planes):
+
+        @pl.when(jnp.logical_and(z + 1 < planes, z - d + 1 >= 0))
+        def _():
+            remote(keys_of(z), keys_of(z), kv_send.at[d], kv_recv.at[d], above, tp).wait_send()
+            remote(mine, mine, up_send.at[d], up_recv.at[d], above, tp).wait_send()
+
+        @pl.when(jnp.logical_and(z > 0, z + d - 1 < planes))
+        def _():
+            remote(mine, mine, down_send.at[d], down_recv.at[d], below, tp).wait_send()
 
     for copy in started:
         copy.wait_send()
@@ -458,67 +553,43 @@
     local = pl.BlockSpec(memory_space=pltpu.VMEM)
     shape = jax.ShapeDtypeStruct
 
-    q_all, kv_all, lift_all, gate_all = pl.pallas_call(
-        functools.partial(spread_kernel, plane, planes, width),
+    span = plane * tok
+    pair = dma((planes + 1,))
+    lift_all, gate_all, normed, halo, stream = pl.pallas_call(
+        functools.partial(front_kernel, plane, planes, width),
         out_shape=(
-            shape((plane * tok, 2 * HD), bf16),
-            shape((count, 4 * HD), bf16),
             shape((count, width), bf16),
             shape((count, width), bf16),
-        ),
-        in_specs=[anywhere] * 7,
-        out_specs=(anywhere,) * 4,
-        scratch_shapes=[
-            dma((7,)), dma((plane, 5)), dma((plane, 5)), dma((planes, 2)), dma((planes, 2)),
-            dma((planes,)), dma((planes,)), dma((planes, plane, 2)), dma((planes, plane, 2)),
-        ],
-        compiler_params=pltpu.CompilerParams(collective_id=0, has_side_effects=True),
-        name="spread",
-    )(query_one, key_one, query_two, key_two, values, lift_weight, gate_weight)
-
-    k_pos = lax.iota(jnp.int32, count)
-    q_pos = z * plane * tok + lax.iota(jnp.int32, plane * tok)
-    visible = k_pos[None, :] // STRETCH <= q_pos[:, None] // STRETCH
-    arrived = k_pos[:, None] < (z + 1) * plane * tok
-    vals = jnp.where(arrived, kv_all[:, 2 * HD :], 0)
-
-    def one_map(index):
-        queries = q_all[:, index * HD : (index + 1) * HD]
-        keys = kv_all[:, index * HD : (index + 1) * HD]
-        scores = jnp.einsum("td,sd->ts", queries, keys, preferred_element_type=f32) * HD**-0.5
-        scores = jnp.where(visible, scores, masked_score)
-        weights = jnp.where(visible, jnp.exp(scores - jnp.max(scores, axis=-1, keepdims=True)), 0.0)
-        total = jnp.sum(weights, axis=-1, keepdims=True)
-        return jnp.dot(weights.astype(bf16), vals, preferred_element_type=f32) / total
-
-    mixed = one_map(0) - mix_weight[p] * one_map(1)
-    head_out = (
-        mixed * lax.rsqrt(jnp.mean(mixed * mixed, axis=-1, keepdims=True) + epsilon) * head_gain
-    ).astype(bf16)
-
-    normed, halo, stream = pl.pallas_call(
-        functools.partial(out_kernel, plane, planes),
-        out_shape=(
             shape((planes, tok, model), bf16),
             shape((planes, 8, model), bf16),
             shape((tok // 2, model), f32),
         ),
-        in_specs=[local] * 4,
-        out_specs=(local,) * 3,
+        in_specs=[anywhere] * 7 + [pl.BlockSpec(memory_space=pltpu.SMEM)] + [local] * 4,
+        out_specs=(anywhere, anywhere, local, local, local),
         scratch_shapes=[
+            pltpu.VMEM((span, 2 * HD), bf16),
+            pltpu.VMEM((count, 4 * HD), bf16),
+            pltpu.VMEM((2, span, HD), f32),
+            pltpu.VMEM((2, span, HD), f32),
+            pltpu.VMEM((2, span, val), f32),
+            pltpu.VMEM((span, val), bf16),
             pltpu.VMEM((plane, tok, val), bf16),
             pltpu.VMEM((tok // 2, model), bf16),
             pltpu.VMEM((tok // 2, model), bf16),
             pltpu.VMEM((8, model), bf16),
-            dma, dma((plane,)), dma((plane,)), dma, dma,
-            dma((planes,)), dma((planes,)), dma((planes,)), dma((planes,)),
-            dma((planes, 2)), dma((planes,)),
+            dma((7,)), dma((plane, 5)), dma((plane, 5)), dma((planes, 2)), dma((planes, 2)),
+            pair, pair, dma((planes, plane, 2)), dma((planes, plane, 2)),
+            dma, dma((plane,)), dma((plane,)), dma, dma, pair, pair, pair, pair,
+            dma((planes,)), dma((planes,)), dma((planes, 2)), dma((planes,)),
         ],
         compiler_params=pltpu.CompilerParams(
-            collective_id=1, has_side_effects=True, vmem_limit_bytes=32 << 20
+            collective_id=0, has_side_effects=True, vmem_limit_bytes=40 << 20
         ),
-        name="project",
-    )(head_out, out_weight, residual, norm_gain.reshape(1, model))
+        name="front",
+    )(
+        query_one, key_one, query_two, key_two, values, lift_weight, gate_weight, mix_weight,
+        head_gain.reshape(1, val), out_weight, residual, norm_gain.reshape(1, model),
+    )
 
     rows = jnp.concatenate([halo, normed], axis=1).reshape(planes * (tok + 8), model)
     lifted = jnp.dot(rows, lift_all, preferred_element_type=f32).astype(bf16)
@@ -545,7 +616,7 @@
             dma, dma((planes,)), dma((planes,)), dma, dma,
         ],
         compiler_params=pltpu.CompilerParams(
-            collective_id=2, has_side_effects=True, vmem_limit_bytes=40 << 20
+            collective_id=1, has_side_effects=True, vmem_limit_bytes=40 << 20
         ),
         name="down",
     )(hidden, down_weight, stream)

time: 175 us -> 176 us (level)
  matrix products: 14 us -> 3.77 us
  local copies, waits for them, and re-layouts: 9.1 us -> 15.7 us
  Pallas kernels: 148 us -> 154 us
    dot_general x4 -> x0, matrix products: 10.2 us -> none  [the longest x2 5.85 us: one_map(): jnp.dot(weights.astype(bf16), vals, preferred_element_type=f32) / total]
    unnamed x27 -> x25, local copies, waits for them, and re-layouts: 7.6 us -> 14.7 us
    pallas_call x1, Pallas kernels: 26.1 us -> 31.3 us  [shorter_routes(): pl.pallas_call(functools.partial(down_kernel, plane, planes, starts), out...]
    pallas_call x2 -> x1, Pallas kernels: 122 us -> 122 us  [shorter_routes(): pl.pallas_call(functools.partial(front_kernel, plane, planes, width), out...]
where the time goes in v2:
time: 176 us; the launch traced here: 174 us
  Pallas kernels  154 us (88%)
  local copies, waits for them, and re-layouts  15.7 us (9%)
  matrix products  3.77 us (2%)
    pallas_call x1, Pallas kernels, shorter_routes(): pl.pallas_call(functools.partial(front_kernel, plane, planes, width), out...  122 us
    pallas_call x1, Pallas kernels, shorter_routes(): pl.pallas_call(functools.partial(down_kernel, plane, planes, starts), out...  31.3 us
    unnamed x25, local copies, waits for them, and re-layouts  14.7 us

profile of v2, /device:TPU:25, one launch (start us, length us, event | category | flops | bytes accessed | tf_op | source)
XLA Modules:
  0.0 174.3 jit_solution(11434165702006661132)
XLA Ops:
  0.0 0.0 copy-start.1
  0.0 1.1 copy-done.1
  1.1 0.0 copy-start.2
  1.1 1.1 copy-done.2
  2.2 0.0 copy-start.3
  2.2 0.9 copy-done.3
  3.2 0.0 copy-start.4
  3.2 0.9 copy-done.4
  4.1 0.0 copy-start.5
  4.1 0.9 copy-done.5
  5.0 0.0 copy-start.6
  5.0 0.9 copy-done.6
  5.9 0.0 copy-start.7
  5.9 0.9 copy-done.7
  6.8 0.0 copy-start.8
  6.8 0.9 copy-done.8
  7.7 0.0 copy-start.9
  7.7 0.7 copy-done.9
  8.4 0.0 copy-start.10
  8.4 0.7 copy-done.10
  9.1 0.7 copy-done.11
  9.8 122.3 %front.1 = (bf16[2048,768]{1,0:T(8,128)(2,1)S(1)}, bf16[2048,768]{1,0:T(8,128)(2,1)S(1)}, bf16[4,128,2048]{2,1,0:T(8,128)(2,1)S(1)}, bf16[4,8,2048]{2,1,0:T(8,128)(2,1)S(1)}, f32[64,2048]{1,0:T(8,128)S(1)}) custom-call(bf16[128,512]{1,0:T(8,128)(2,1)S(1)} %copy-done.5, bf16[128,512]{1,0:T(8,128)(2,1)S(1)} %copy-done.6, bf16[128,512]{1,0:T(8,128)(2,1)S(1)} %copy-done.7, ...), custom_call_target="tpu_custom_call" | custom-call | tf_op jit(solution)/shard_map/front/pallas_call | solution.py:558
  132.0 0.3 pad_maximum_fusion
  132.3 1.9 %convolution_convert_fusion.1 = bf16[544,768]{1,0:T(8,128)(2,1)S(1)} fusion(bf16[544,2048]{1,0:T(8,128)(2,1)S(1)} %bitcast.12, bf16[2048,768]{1,0:T(8,128)(2,1)S(1)} %get-tuple-element.12), kind=kOutput, calls=%fused_computation.8 | convolution fusion | flops 1711693824 | bytes 6209536 | tf_op jit(solution)/shard_map/dot_general | solution.py:596
  134.2 0.1 convert.1
  134.3 1.9 %convolution_convert_fusion = bf16[544,768]{1,0:T(8,128)(2,1)S(1)} fusion(bf16[544,2048]{1,0:T(8,128)(2,1)S(1)} %bitcast.13, bf16[2048,768]{1,0:T(8,128)(2,1)S(1)} %get-tuple-element.13), kind=kOutput, calls=%fused_computation.7 | convolution fusion | flops 1711693824 | bytes 6209536 | tf_op jit(solution)/shard_map/dot_general | solution.py:595
  136.2 0.9 dynamic-slice_reduce_fusion.2
  137.2 0.9 multiply_convert_fusion.hidden
  138.0 0.0 copy-start
  138.0 4.3 %copy-done = bf16[2816,2048]{1,0:T(8,128)(2,1)S(1)} copy-done((bf16[2816,2048]{1,0:T(8,128)(2,1)S(1)}, bf16[2816,2048]{1,0:T(8,128)(2,1)}, u32[]{:S(2)}) %copy-start) | copy-done | bytes 11534360
  142.3 31.3 %down.1 = bf16[64,2048]{1,0:T(8,128)(2,1)S(1)} custom-call(bf16[4,128,768]{2,1,0:T(8,128)(2,1)S(1)} %multiply_convert_fusion.hidden, bf16[2816,2048]{1,0:T(8,128)(2,1)S(1)} %copy-done, f32[64,2048]{1,0:T(8,128)S(1)} %get-tuple-element.14.stream), custom_call_target="tpu_custom_call" | custom-call | tf_op jit(solution)/shard_map/down/pallas_call | solution.py:606
  173.6 0.7 copy.16
  (1 shorter events, 0.0 us)
Async XLA Ops:
  0.0 1.1 copy-start.1
  1.1 1.1 copy-start.2
  2.2 0.9 copy-start.3
  3.2 0.9 copy-start.4
  4.1 0.9 copy-start.5
  5.0 0.9 copy-start.6
  5.9 0.9 copy-start.7
  6.8 0.9 copy-start.8
  7.7 0.7 copy-start.9
  8.4 0.7 copy-start.10
  9.1 0.7 copy-start.11
  138.0 4.3 %copy-start = (bf16[2816,2048]{1,0:T(8,128)(2,1)S(1)}, bf16[2816,2048]{1,0:T(8,128)(2,1)}, u32[]{:S(2)}) copy-start(bf16[2816,2048]{1,0:T(8,128)(2,1)} %weight.1) | copy-start | bytes 34603012

commit v3 on v2

--- a/solution.py
+++ b/solution.py
@@ -150,10 +150,10 @@
 
 
 def front_kernel(
-    plane, planes, width, q1, k1, q2, k2, v, lift, gate, mix_weight, head_gain, out_weight, residual,
+    plane, planes, width, q1, k1, q2, k2, v, lift, gate, mix_weight, head_gain, out_hbm, residual_hbm,
     gain,
     lift_all, gate_all, normed, halo, stream,
-    q_all, kv_all, peaks, totals, sums, head_out, heads, part, part_in, tail,
+    q_all, kv_all, peaks, totals, sums, head_out, heads, part, part_in, tail, out_weight, residual,
     own_sem, a_send, a_recv, w_send, w_recv, kv_send, kv_recv, g_send, g_recv,
     b_own, b_send, b_recv, t_send, t_recv, up_send, up_recv, down_send, down_recv,
     f_send, f_recv, h_send, h_recv,
@@ -201,6 +201,10 @@
     ]
     for copy in own:
         copy.start()
+    loads = [
+        pltpu.make_async_copy(out_hbm, out_weight, own_sem.at[7]),
+        pltpu.make_async_copy(residual_hbm, residual, own_sem.at[8]),
+    ]
     pl.semaphore_wait(barrier, len(peers) + 2 * planes * tp)
     for d in range(1, plane):
         there = (p + d) % plane
@@ -209,15 +213,30 @@
             copy.start()
             started.append(copy)
 
-    def send_weights(d):
+    lanes = {}
+    for d in range(1, planes):
         there = (z + d) % planes
-        for m, (src, dst) in enumerate(weights):
-            copy = remote(
+        lanes[d] = [
+            remote(
                 src.at[:, units(there)], dst.at[block_of(sp, tok), :],
                 w_send.at[d, m], w_recv.at[d, m], there * plane + p, tp,
             )
-            copy.start()
-            started.append(copy)
+            for m, (src, dst) in enumerate(weights)
+        ]
+        started.extend(lanes[d])
+
+    def send_weights(early):
+        for d in range(planes - 1, 0, -1):
+            if d == planes - 1:
+                if early:
+                    for copy in lanes[d]:
+                        copy.start()
+                continue
+
+            @pl.when((z + d >= planes) if early else (z + d < planes))
+            def _():
+                for copy in lanes[d]:
+                    copy.start()
 
     def share_weights(d):
         source = (z + planes - d) % planes * plane + p
@@ -236,10 +255,9 @@
                 copy.start()
                 started.append(copy)
 
-    if planes > 2:
-        send_weights(planes - 1)
+    send_weights(True)
     share_weights(0)
-    for copy in own_weights:
+    for copy in own_weights + loads:
         copy.start()
     for copy in own:
         copy.wait()
@@ -305,17 +323,14 @@
             def _():
                 remote(here, here, kv_send.at[d + 1], kv_recv.at[d + 1], above, tp).start()
 
-        if d < planes - 1:
-            send_weights(planes - 1 - d)
-        elif planes == 2:
-            send_weights(1)
-
         @pl.when(z - d >= 0)
         def _():
             attend((z + planes - d) % planes, False)
 
-        if d == 1 and planes > 2:
+        if d == 1:
             share_weights(planes - 1)
+
+    send_weights(False)
 
     @pl.loop(0, plane)
     def _(chunk):
@@ -344,6 +359,8 @@
             heads.at[there], heads.at[there], b_send.at[d], b_recv.at[d], z * plane + there, tp
         ).wait_recv()
 
+    for copy in loads:
+        copy.wait()
     columns = 512
 
     def product(which, at):
@@ -397,6 +414,8 @@
                     tail, halo.at[zone], h_send.at[s, t], h_recv.at[zone], s * plane + after, t
                 ).start()
 
+    for d in range(planes - 2, 0, -1):
+        share_weights(d)
     for d in range(1, planes):
 
         @pl.when(z - d >= 0)
@@ -421,11 +440,6 @@
 
             at = planes - d
             remote(theirs, theirs, f_send.at[at], f_recv.at[at], sp, other).start()
-
-        if d < planes - 1:
-            share_weights(planes - 1 - d)
-        elif planes == 2:
-            share_weights(1)
 
     for d in range(planes):
         theirs = tokens(z + planes - d, other)
@@ -475,13 +489,22 @@
 
 def down_kernel(
     plane, planes, starts, hidden, weight, stream, out,
-    units, total_buf, part, part_in, own_sem, a_send, a_recv, t_send, t_recv,
+    held, units, total, part, part_in, l_sem, own_sem, a_send, a_recv, t_send, t_recv,
 ):
     sp, tp = lax.axis_index("sp"), lax.axis_index("tp")
     z, p = sp // plane, sp % plane
     other = 1 - tp
-    tok = units.shape[1]
+    tok, width = units.shape[1:]
     half = tok // 2
+    tiles = weight.shape[0] // 128
+
+    def load(d):
+        at = (z + planes - d) % planes
+        first = pl.multiple_of(at * tiles // planes * 128, 128)
+        return pltpu.make_async_copy(weight.at[pl.ds(first, width), :], held.at[d], l_sem.at[d])
+
+    for d in range(planes):
+        load(d).start()
     greet([((z + d) % planes * plane + p, tp) for d in range(1, planes)] + [(sp, other)])
     started = []
     own = pltpu.make_async_copy(hidden.at[z], units.at[z], own_sem)
@@ -493,41 +516,31 @@
         )
         copy.start()
         started.append(copy)
-    own.wait()
-    for d in range(1, planes):
+    columns = 512
+    order = [0] + list(range(1, planes))
+    for d in order:
         there = (z + planes - d) % planes
-        remote(
-            units.at[there], units.at[there], a_send.at[d], a_recv.at[d], sp, other
-        ).wait_recv()
-    model = weight.shape[1]
-    columns = 256
-
-    def product(which, at):
-        total = None
-        for s in range(planes):
-            term = jnp.dot(
-                units[s, block_of(which, half), 0 : starts[s + 1] - starts[s]],
-                weight[starts[s] : starts[s + 1], block_of(at, columns)],
-                preferred_element_type=jnp.float32,
-            )
-            total = term if total is None else total + term
-        return total.astype(jnp.bfloat16)
-
-    @pl.loop(0, model // columns)
-    def _(at):
-        part[:, block_of(at, columns)] = product(other, at)
-
+        load(d).wait()
+        if d:
+            remote(
+                units.at[there], units.at[there], a_send.at[d], a_recv.at[d], sp, other
+            ).wait_recv()
+        else:
+            own.wait()
+
+        @pl.loop(0, weight.shape[1] // columns)
+        def _(at):
+            here = block_of(at, columns)
+            term = jnp.dot(units[there], held[d, :, here], preferred_element_type=jnp.float32)
+            total[:, here] = term if d == 0 else total[:, here] + term
+
+    part[...] = total[block_of(other, half), :].astype(jnp.bfloat16)
     swap = remote(part, part_in, t_send, t_recv, sp, other)
     swap.start()
     started.append(swap)
-
-    @pl.loop(0, model // columns)
-    def _(at):
-        here = block_of(at, columns)
-        total_buf[:, here] = stream[:, here] + product(tp, at).astype(jnp.float32)
-
+    mine = total[block_of(tp, half), :].astype(jnp.bfloat16).astype(jnp.float32)
     swap.wait_recv()
-    out[...] = (total_buf[...] + part_in[...].astype(jnp.float32)).astype(out.dtype)
+    out[...] = (stream[...] + (mine + part_in[...].astype(jnp.float32))).astype(out.dtype)
     for copy in started:
         copy.wait_send()
 
@@ -564,7 +577,7 @@
             shape((planes, 8, model), bf16),
             shape((tok // 2, model), f32),
         ),
-        in_specs=[anywhere] * 7 + [pl.BlockSpec(memory_space=pltpu.SMEM)] + [local] * 4,
+        in_specs=[anywhere] * 7 + [pl.BlockSpec(memory_space=pltpu.SMEM)] + [local, anywhere, anywhere, local],
         out_specs=(anywhere, anywhere, local, local, local),
         scratch_shapes=[
             pltpu.VMEM((span, 2 * HD), bf16),
@@ -577,13 +590,15 @@
             pltpu.VMEM((tok // 2, model), bf16),
             pltpu.VMEM((tok // 2, model), bf16),
             pltpu.VMEM((8, model), bf16),
-            dma((7,)), dma((plane, 5)), dma((plane, 5)), dma((planes, 2)), dma((planes, 2)),
+            pltpu.VMEM(out_weight.shape, bf16),
+            pltpu.VMEM(residual.shape, bf16),
+            dma((9,)), dma((plane, 5)), dma((plane, 5)), dma((planes, 2)), dma((planes, 2)),
             pair, pair, dma((planes, plane, 2)), dma((planes, plane, 2)),
             dma, dma((plane,)), dma((plane,)), dma, dma, pair, pair, pair, pair,
             dma((planes,)), dma((planes,)), dma((planes, 2)), dma((planes,)),
         ],
         compiler_params=pltpu.CompilerParams(
-            collective_id=0, has_side_effects=True, vmem_limit_bytes=40 << 20
+            collective_id=0, has_side_effects=True, vmem_limit_bytes=62 << 20
         ),
         name="front",
     )(
@@ -602,21 +617,24 @@
         at = 8 - (WIDTH - 1) + index
         conv = conv + taps[index] * gated[:, at : at + tok]
     hidden = (jax.nn.silu(conv) * lifted).astype(bf16)
+    mine = (z + 1) * tiles // planes * 128 - z * tiles // planes * 128
+    hidden = jnp.where(lax.iota(jnp.int32, width) < mine, hidden, 0)
 
     return pl.pallas_call(
         functools.partial(down_kernel, plane, planes, starts),
         out_shape=shape((tok // 2, model), bf16),
-        in_specs=[local] * 3,
+        in_specs=[local, anywhere, local],
         out_specs=local,
         scratch_shapes=[
+            pltpu.VMEM((planes, width, model), bf16),
             pltpu.VMEM((planes, tok, width), bf16),
-            pltpu.VMEM((tok // 2, model), f32),
+            pltpu.VMEM((tok, model), f32),
             pltpu.VMEM((tok // 2, model), bf16),
             pltpu.VMEM((tok // 2, model), bf16),
-            dma, dma((planes,)), dma((planes,)), dma, dma,
+            dma((planes,)), dma, dma((planes,)), dma((planes,)), dma, dma,
         ],
         compiler_params=pltpu.CompilerParams(
-            collective_id=1, has_side_effects=True, vmem_limit_bytes=40 << 20
+            collective_id=1, has_side_effects=True, vmem_limit_bytes=62 << 20
         ),
         name="down",
     )(hidden, down_weight, stream)

time: 176 us -> 160 us (0.909)
  local copies, waits for them, and re-layouts: 15.7 us -> 3.25 us
  Pallas kernels: 154 us -> 148 us
  other arithmetic: 1.23 us -> 3.8 us
    unnamed x25 -> x5, local copies, waits for them, and re-layouts: 14.7 us -> 2.33 us
    pallas_call x1, Pallas kernels: 31.3 us -> 26.6 us  [shorter_routes(): pl.pallas_call(functools.partial(down_kernel, plane, planes, starts), out...]
    select_n x0 -> x1, other arithmetic: none -> 1.78 us  [shorter_routes(): hidden = jnp.where(lax.iota(jnp.int32, width) < mine, hidden, 0)]
where the time goes in v3:
time: 160 us; the launch traced here: 159 us
  Pallas kernels  148 us (92%)
  matrix products  3.81 us (2%)
  other arithmetic  3.8 us (2%)
  local copies, waits for them, and re-layouts  3.25 us (2%)
    pallas_call x1, Pallas kernels, shorter_routes(): pl.pallas_call(functools.partial(front_kernel, plane, planes, width), out...  122 us
    pallas_call x1, Pallas kernels, shorter_routes(): pl.pallas_call(functools.partial(down_kernel, plane, planes, starts), out...  26.6 us

profile of v3, /device:TPU:25, one launch (start us, length us, event | category | flops | bytes accessed | tf_op | source)
XLA Modules:
  0.0 159.3 jit_solution(8019129822077328470)
XLA Ops:
  0.0 121.8 %front.1 = (bf16[2048,768]{1,0:T(8,128)(2,1)}, bf16[2048,768]{1,0:T(8,128)(2,1)}, bf16[4,128,2048]{2,1,0:T(8,128)(2,1)}, bf16[4,8,2048]{2,1,0:T(8,128)(2,1)}, f32[64,2048]{1,0:T(8,128)}) custom-call(bf16[128,512]{1,0:T(8,128)(2,1)} %q1.1, bf16[128,512]{1,0:T(8,128)(2,1)} %k1.1, bf16[128,512]{1,0:T(8,128)(2,1)} %q2.1, bf16[128,512]{1,0:T(8,128)(2,1)} %k2.1, ...), custom_call_target="tpu_custom_call" | custom-call | tf_op jit(solution)/shard_map/front/pallas_call | solution.py:571
  121.8 0.0 copy-start.1
  121.8 1.9 %pad_maximum_fusion = bf16[4,136,2048]{2,1,0:T(8,128)(2,1)S(1)} fusion(bf16[4,128,2048]{2,1,0:T(8,128)(2,1)} %get-tuple-element.11, bf16[4,8,2048]{2,1,0:T(8,128)(2,1)} %get-tuple-element.10), kind=kLoop, calls=%fused_computation | loop fusion | flops 4456448 | bytes 4456448 | tf_op jit(solution)/shard_map/concatenate | solution.py:609
  123.7 0.7 copy-done.1
  124.4 0.0 copy-start
  124.4 1.9 %convolution_convert_fusion = bf16[544,768]{1,0:T(8,128)(2,1)S(1)} fusion(bf16[544,2048]{1,0:T(8,128)(2,1)S(1)} %bitcast.10, bf16[2048,768]{1,0:T(8,128)(2,1)S(1)} %copy-done.1), kind=kOutput, calls=%fused_computation.7 | convolution fusion | flops 1711693824 | bytes 6209536 | tf_op jit(solution)/shard_map/dot_general | solution.py:610
  126.3 0.0 copy-done
  126.3 1.9 %convolution_convert_fusion.1 = bf16[544,768]{1,0:T(8,128)(2,1)S(1)} fusion(bf16[544,2048]{1,0:T(8,128)(2,1)S(1)} %bitcast.11, bf16[2048,768]{1,0:T(8,128)(2,1)S(1)} %copy-done), kind=kOutput, calls=%fused_computation.8 | convolution fusion | flops 1711693824 | bytes 6209536 | tf_op jit(solution)/shard_map/dot_general | solution.py:611
  128.2 0.1 convert.1
  128.3 0.9 dynamic-slice_reduce_fusion.2
  129.3 1.8 %broadcast_select_fusion.hidden = bf16[4,128,768]{2,1,0:T(8,128)(2,1)} fusion(pred[768]{0:T(1024)(128)(4,1)S(1)} %iota_compare_fusion, bf16[4,136,768]{2,1,0:T(8,128)(2,1)S(1)} %bitcast.13, f32[4,136,768]{2,1,0:T(8,128)S(1)} %convert.1, f32[768]{0:T(1024)S(1)} %get-tuple-element.17, f32[768]{0:T(1024)S(1)} %get-tuple-element.16, f32[768]{0:T(1024)S(1)} %get-tuple-element.15), kind=kLoop, calls=%fused_computation.9 | loop fusion | flops 5111808 | bytes 6301440 | tf_op jit(solution)/shard_map/jit(_where)/select_n | solution.py:621
  131.0 26.6 %down.1 = bf16[64,2048]{1,0:T(8,128)(2,1)} custom-call(bf16[4,128,768]{2,1,0:T(8,128)(2,1)} %broadcast_select_fusion.hidden, bf16[2816,2048]{1,0:T(8,128)(2,1)} %weight.1, f32[64,2048]{1,0:T(8,128)} %get-tuple-element.14.stream), custom_call_target="tpu_custom_call" | custom-call | tf_op jit(solution)/shard_map/down/pallas_call | solution.py:623
  157.6 1.7 %copy.16 = bf16[64,2048]{1,0:T(8,128)(2,1)} copy(bf16[64,2048]{1,0:T(8,128)(2,1)} %down.1) | data formatting | bytes 524288
  (1 shorter events, 0.0 us)
Async XLA Ops:
  121.8 2.6 %copy-start.1 = (bf16[2048,768]{1,0:T(8,128)(2,1)S(1)}, bf16[2048,768]{1,0:T(8,128)(2,1)}, u32[]{:S(2)}) copy-start(bf16[2048,768]{1,0:T(8,128)(2,1)} %get-tuple-element.13) | copy-start | bytes 9437188
  124.4 1.9 %copy-start = (bf16[2048,768]{1,0:T(8,128)(2,1)S(1)}, bf16[2048,768]{1,0:T(8,128)(2,1)}, u32[]{:S(2)}) copy-start(bf16[2048,768]{1,0:T(8,128)(2,1)} %get-tuple-element.12) | copy-start | bytes 9437188

commit v4 on v3

--- a/solution.py
+++ b/solution.py
@@ -206,12 +206,15 @@
         pltpu.make_async_copy(residual_hbm, residual, own_sem.at[8]),
     ]
     pl.semaphore_wait(barrier, len(peers) + 2 * planes * tp)
-    for d in range(1, plane):
-        there = (p + d) % plane
-        for n, (src, dst) in enumerate(piece(there, sp)):
-            copy = remote(src, dst, a_send.at[d, n], a_recv.at[d, n], z * plane + there, tp)
-            copy.start()
-            started.append(copy)
+    for part_of in ((0, 1, 2), (3, 4)):
+        for d in range(1, plane):
+            there = (p + d) % plane
+            pairs = piece(there, sp)
+            for n in part_of:
+                src, dst = pairs[n]
+                copy = remote(src, dst, a_send.at[d, n], a_recv.at[d, n], z * plane + there, tp)
+                copy.start()
+                started.append(copy)
 
     lanes = {}
     for d in range(1, planes):
@@ -227,16 +230,20 @@
 
     def send_weights(early):
         for d in range(planes - 1, 0, -1):
-            if d == planes - 1:
-                if early:
-                    for copy in lanes[d]:
-                        copy.start()
-                continue
 
             @pl.when((z + d >= planes) if early else (z + d < planes))
             def _():
                 for copy in lanes[d]:
                     copy.start()
+
+    square = plane == 4
+    direct = (1, 2) if square else range(1, plane)
+
+    def partner(e):
+        if not square:
+            return (p + e) % plane
+        flips = {1: p + 1 - 2 * (p % 2), 2: (p + 2) % 4, 3: 3 - p}
+        return flips[e]
 
     def share_weights(d):
         source = (z + planes - d) % planes * plane + p
@@ -247,33 +254,63 @@
                     dst.at[rows, :], dst.at[rows, :], w_send.at[d, m], w_recv.at[d, m], source, tp
                 ).wait_recv()
             src = dst.at[rows, :] if d else weights[m][0].at[:, units(z)]
-            for e in range(1, plane):
+            for e in direct:
                 copy = remote(
                     src, dst.at[rows, :], g_send.at[d, e, m], g_recv.at[d, e, m],
-                    z * plane + (p + e) % plane, tp,
+                    z * plane + partner(e), tp,
                 )
                 copy.start()
                 started.append(copy)
+
+    def pass_weights(d):
+        for m, dst in enumerate((lift_all, gate_all)):
+            for e in direct:
+                there = partner(e) if square else (p + plane - e) % plane
+                rows = block_of((z + planes - d) % planes * plane + there, tok)
+                block = dst.at[rows, :]
+                remote(
+                    block, block, g_send.at[d, e, m], g_recv.at[d, e, m], z * plane + there, tp
+                ).wait_recv()
+                if square and e == m + 1:
+                    copy = remote(
+                        block, block, g_send.at[d, 3, m], g_recv.at[d, 3, m],
+                        z * plane + partner(3 - e), tp,
+                    )
+                    copy.start()
+                    started.append(copy)
 
     send_weights(True)
     share_weights(0)
     for copy in own_weights + loads:
         copy.start()
-    for copy in own:
+    span = plane * tok
+
+    def keys_of(index, e):
+        return kv_all.at[block_of(index * plane + (p + plane - e) % plane, tok), :]
+
+    def arrival(e, which):
+        source = z * plane + (p + plane - e) % plane
+        pairs = piece(p, source)
+        for n in which:
+            src, dst = pairs[n]
+            remote(src, dst, a_send.at[e, n], a_recv.at[e, n], source, tp).wait_recv()
+
+    for e in range(plane):
+        if e:
+            arrival(e, (0, 1, 2))
+        else:
+            for copy in own[:3]:
+                copy.wait()
+
+        @pl.when(z + 1 < planes)
+        def _():
+            block = keys_of(z, e)
+            remote(block, block, kv_send.at[1, e], kv_recv.at[1, e], above, tp).start()
+
+    for copy in own[3:]:
         copy.wait()
-    for d in range(1, plane):
-        source = z * plane + (p + plane - d) % plane
-        for n, (src, dst) in enumerate(piece(p, source)):
-            remote(src, dst, a_send.at[d, n], a_recv.at[d, n], source, tp).wait_recv()
-
-    span = plane * tok
-
-    def keys_of(index):
-        return kv_all.at[block_of(index, span), :]
-
-    @pl.when(z + 1 < planes)
-    def _():
-        remote(keys_of(z), keys_of(z), kv_send.at[1], kv_recv.at[1], above, tp).start()
+    for e in range(1, plane):
+        arrival(e, (3, 4))
 
     def attend(source, first):
         @pl.loop(0, plane)
@@ -313,22 +350,25 @@
 
     attend(z, True)
     for d in range(1, planes):
-        here = keys_of((z + planes - d) % planes)
 
         @pl.when(z - d >= 0)
         def _():
-            remote(here, here, kv_send.at[d], kv_recv.at[d], below, tp).wait_recv()
-
-            @pl.when(z + 1 < planes)
-            def _():
-                remote(here, here, kv_send.at[d + 1], kv_recv.at[d + 1], above, tp).start()
+            for e in range(plane):
+                here = keys_of((z + planes - d) % planes, e)
+                remote(here, here, kv_send.at[d, e], kv_recv.at[d, e], below, tp).wait_recv()
+
+                @pl.when(z + 1 < planes)
+                def _():
+                    remote(
+                        here, here, kv_send.at[d + 1, e], kv_recv.at[d + 1, e], above, tp
+                    ).start()
 
         @pl.when(z - d >= 0)
         def _():
             attend((z + planes - d) % planes, False)
 
         if d == 1:
-            share_weights(planes - 1)
+            pass_weights(0)
 
     send_weights(False)
 
@@ -353,6 +393,7 @@
         copy.start()
         started.append(copy)
     own.wait()
+    share_weights(planes - 1)
     for d in range(1, plane):
         there = (p + plane - d) % plane
         remote(
@@ -416,6 +457,7 @@
 
     for d in range(planes - 2, 0, -1):
         share_weights(d)
+        pass_weights(d + 1)
     for d in range(1, planes):
 
         @pl.when(z - d >= 0)
@@ -454,11 +496,12 @@
         def _():
             halo[s] = jnp.zeros(halo.shape[1:], halo.dtype)
 
+    pass_weights(1)
     for copy in own_weights:
         copy.wait()
     for d in range(planes):
-        for e in range(1, plane):
-            there = (p + plane - e) % plane
+        for e in (3,) if square else ():
+            there = partner(e)
             rows = block_of((z + planes - d) % planes * plane + there, tok)
             for m, dst in enumerate((lift_all, gate_all)):
                 remote(
@@ -476,7 +519,9 @@
 
         @pl.when(jnp.logical_and(z + 1 < planes, z - d + 1 >= 0))
         def _():
-            remote(keys_of(z), keys_of(z), kv_send.at[d], kv_recv.at[d], above, tp).wait_send()
+            for e in range(plane):
+                block = keys_of(z, e)
+                remote(block, block, kv_send.at[d, e], kv_recv.at[d, e], above, tp).wait_send()
             remote(mine, mine, up_send.at[d], up_recv.at[d], above, tp).wait_send()
 
         @pl.when(jnp.logical_and(z > 0, z + d - 1 < planes))
@@ -593,7 +638,7 @@
             pltpu.VMEM(out_weight.shape, bf16),
             pltpu.VMEM(residual.shape, bf16),
             dma((9,)), dma((plane, 5)), dma((plane, 5)), dma((planes, 2)), dma((planes, 2)),
-            pair, pair, dma((planes, plane, 2)), dma((planes, plane, 2)),
+            dma((planes + 1, plane)), dma((planes + 1, plane)), dma((planes, plane, 2)), dma((planes, plane, 2)),
             dma, dma((plane,)), dma((plane,)), dma, dma, pair, pair, pair, pair,
             dma((planes,)), dma((planes,)), dma((planes, 2)), dma((planes,)),
         ],

time: 160 us -> 152 us (0.950)
  Pallas kernels: 148 us -> 141 us
    pallas_call x1, Pallas kernels: 122 us -> 114 us  [shorter_routes(): pl.pallas_call(functools.partial(front_kernel, plane, planes, width), out...]
where the time goes in v4:
time: 152 us
  Pallas kernels  141 us (93%)
  matrix products  3.81 us (3%)
  other arithmetic  3.8 us (2%)
  local copies, waits for them, and re-layouts  3.25 us (2%)
    pallas_call x1, Pallas kernels, shorter_routes(): pl.pallas_call(functools.partial(front_kernel, plane, planes, width), out...  114 us
    pallas_call x1, Pallas kernels, shorter_routes(): pl.pallas_call(functools.partial(down_kernel, plane, planes, starts), out...  26.6 us

profile of v4, /device:TPU:25, one launch (start us, length us, event | category | flops | bytes accessed | tf_op | source)
XLA Modules:
  0.0 151.8 jit_solution(16157195601355342957)
XLA Ops:
  0.0 114.3 %front.1 = (bf16[2048,768]{1,0:T(8,128)(2,1)}, bf16[2048,768]{1,0:T(8,128)(2,1)}, bf16[4,128,2048]{2,1,0:T(8,128)(2,1)}, bf16[4,8,2048]{2,1,0:T(8,128)(2,1)}, f32[64,2048]{1,0:T(8,128)}) custom-call(bf16[128,512]{1,0:T(8,128)(2,1)} %q1.1, bf16[128,512]{1,0:T(8,128)(2,1)} %k1.1, bf16[128,512]{1,0:T(8,128)(2,1)} %q2.1, bf16[128,512]{1,0:T(8,128)(2,1)} %k2.1, ...), custom_call_target="tpu_custom_call" | custom-call | tf_op jit(solution)/shard_map/front/pallas_call | solution.py:616
  114.3 0.0 copy-start.1
  114.3 1.9 %pad_maximum_fusion = bf16[4,136,2048]{2,1,0:T(8,128)(2,1)S(1)} fusion(bf16[4,128,2048]{2,1,0:T(8,128)(2,1)} %get-tuple-element.11, bf16[4,8,2048]{2,1,0:T(8,128)(2,1)} %get-tuple-element.10), kind=kLoop, calls=%fused_computation | loop fusion | flops 4456448 | bytes 4456448 | tf_op jit(solution)/shard_map/concatenate | solution.py:654
  116.2 0.7 copy-done.1
  116.9 0.0 copy-start
  116.9 1.9 %convolution_convert_fusion = bf16[544,768]{1,0:T(8,128)(2,1)S(1)} fusion(bf16[544,2048]{1,0:T(8,128)(2,1)S(1)} %bitcast.10, bf16[2048,768]{1,0:T(8,128)(2,1)S(1)} %copy-done.1), kind=kOutput, calls=%fused_computation.7 | convolution fusion | flops 1711693824 | bytes 6209536 | tf_op jit(solution)/shard_map/dot_general | solution.py:655
  118.8 0.0 copy-done
  118.8 1.9 %convolution_convert_fusion.1 = bf16[544,768]{1,0:T(8,128)(2,1)S(1)} fusion(bf16[544,2048]{1,0:T(8,128)(2,1)S(1)} %bitcast.11, bf16[2048,768]{1,0:T(8,128)(2,1)S(1)} %copy-done), kind=kOutput, calls=%fused_computation.8 | convolution fusion | flops 1711693824 | bytes 6209536 | tf_op jit(solution)/shard_map/dot_general | solution.py:656
  120.7 0.1 convert.1
  120.9 0.9 dynamic-slice_reduce_fusion.2
  121.8 1.8 %broadcast_select_fusion.hidden = bf16[4,128,768]{2,1,0:T(8,128)(2,1)} fusion(pred[768]{0:T(1024)(128)(4,1)S(1)} %iota_compare_fusion, bf16[4,136,768]{2,1,0:T(8,128)(2,1)S(1)} %bitcast.13, f32[4,136,768]{2,1,0:T(8,128)S(1)} %convert.1, f32[768]{0:T(1024)S(1)} %get-tuple-element.17, f32[768]{0:T(1024)S(1)} %get-tuple-element.16, f32[768]{0:T(1024)S(1)} %get-tuple-element.15), kind=kLoop, calls=%fused_computation.9 | loop fusion | flops 5111808 | bytes 6301440 | tf_op jit(solution)/shard_map/jit(_where)/select_n | solution.py:666
  123.6 26.6 %down.1 = bf16[64,2048]{1,0:T(8,128)(2,1)} custom-call(bf16[4,128,768]{2,1,0:T(8,128)(2,1)} %broadcast_select_fusion.hidden, bf16[2816,2048]{1,0:T(8,128)(2,1)} %weight.1, f32[64,2048]{1,0:T(8,128)} %get-tuple-element.14.stream), custom_call_target="tpu_custom_call" | custom-call | tf_op jit(solution)/shard_map/down/pallas_call | solution.py:668
  150.2 1.7 %copy.16 = bf16[64,2048]{1,0:T(8,128)(2,1)} copy(bf16[64,2048]{1,0:T(8,128)(2,1)} %down.1) | data formatting | bytes 524288
  (1 shorter events, 0.0 us)
Async XLA Ops:
  114.3 2.6 %copy-start.1 = (bf16[2048,768]{1,0:T(8,128)(2,1)S(1)}, bf16[2048,768]{1,0:T(8,128)(2,1)}, u32[]{:S(2)}) copy-start(bf16[2048,768]{1,0:T(8,128)(2,1)} %get-tuple-element.13) | copy-start | bytes 9437188
  116.9 1.9 %copy-start = (bf16[2048,768]{1,0:T(8,128)(2,1)S(1)}, bf16[2048,768]{1,0:T(8,128)(2,1)}, u32[]{:S(2)}) copy-start(bf16[2048,768]{1,0:T(8,128)(2,1)} %get-tuple-element.12) | copy-start | bytes 9437188

commit v5 on v4

--- a/solution.py
+++ b/solution.py
@@ -245,22 +245,40 @@
         flips = {1: p + 1 - 2 * (p % 2), 2: (p + 2) % 4, 3: 3 - p}
         return flips[e]
 
-    def share_weights(d):
+    def share_weights(d, condition=None, record=True):
         source = (z + planes - d) % planes * plane + p
         rows = block_of(source, tok)
+        arrivals, copies = [], []
         for m, dst in enumerate((lift_all, gate_all)):
+            block = dst.at[rows, :]
             if d:
-                remote(
-                    dst.at[rows, :], dst.at[rows, :], w_send.at[d, m], w_recv.at[d, m], source, tp
-                ).wait_recv()
-            src = dst.at[rows, :] if d else weights[m][0].at[:, units(z)]
-            for e in direct:
-                copy = remote(
-                    src, dst.at[rows, :], g_send.at[d, e, m], g_recv.at[d, e, m],
-                    z * plane + partner(e), tp,
+                arrivals.append(
+                    remote(block, block, w_send.at[d, m], w_recv.at[d, m], source, tp)
                 )
-                copy.start()
-                started.append(copy)
+            src = block if d else weights[m][0].at[:, units(z)]
+            copies.append(
+                [
+                    remote(
+                        src, block, g_send.at[d, e, m], g_recv.at[d, e, m],
+                        z * plane + partner(e), tp,
+                    )
+                    for e in direct
+                ]
+            )
+
+        def run():
+            for m in range(2):
+                if d:
+                    arrivals[m].wait_recv()
+                for copy in copies[m]:
+                    copy.start()
+
+        if condition is None:
+            run()
+        else:
+            pl.when(condition)(run)
+        if record:
+            started.extend(copies[0] + copies[1])
 
     def pass_weights(d):
         for m, dst in enumerate((lift_all, gate_all)):
@@ -393,7 +411,7 @@
         copy.start()
         started.append(copy)
     own.wait()
-    share_weights(planes - 1)
+    share_weights(planes - 1, z < planes - 1)
     for d in range(1, plane):
         there = (p + plane - d) % plane
         remote(
@@ -455,6 +473,7 @@
                     tail, halo.at[zone], h_send.at[s, t], h_recv.at[zone], s * plane + after, t
                 ).start()
 
+    share_weights(planes - 1, z == planes - 1, False)
     for d in range(planes - 2, 0, -1):
         share_weights(d)
         pass_weights(d + 1)

time: 152 us -> 157 us (1.033)
  Pallas kernels: 141 us -> 145 us
    pallas_call x1, Pallas kernels: 114 us -> 119 us  [shorter_routes(): pl.pallas_call(functools.partial(front_kernel, plane, planes, width), out...]
where the time goes in v5:
time: 157 us; the launch traced here: 156 us
  Pallas kernels  145 us (92%)
  matrix products  3.81 us (2%)
  other arithmetic  3.8 us (2%)
  local copies, waits for them, and re-layouts  3.25 us (2%)
    pallas_call x1, Pallas kernels, shorter_routes(): pl.pallas_call(functools.partial(front_kernel, plane, planes, width), out...  119 us
    pallas_call x1, Pallas kernels, shorter_routes(): pl.pallas_call(functools.partial(down_kernel, plane, planes, starts), out...  26.6 us

profile of v5, /device:TPU:25, one launch (start us, length us, event | category | flops | bytes accessed | tf_op | source)
XLA Modules:
  0.0 156.4 jit_solution(4080975560229717519)
XLA Ops:
  0.0 118.9 %front.1 = (bf16[2048,768]{1,0:T(8,128)(2,1)}, bf16[2048,768]{1,0:T(8,128)(2,1)}, bf16[4,128,2048]{2,1,0:T(8,128)(2,1)}, bf16[4,8,2048]{2,1,0:T(8,128)(2,1)}, f32[64,2048]{1,0:T(8,128)}) custom-call(bf16[128,512]{1,0:T(8,128)(2,1)} %q1.1, bf16[128,512]{1,0:T(8,128)(2,1)} %k1.1, bf16[128,512]{1,0:T(8,128)(2,1)} %q2.1, bf16[128,512]{1,0:T(8,128)(2,1)} %k2.1, ...), custom_call_target="tpu_custom_call" | custom-call | tf_op jit(solution)/shard_map/front/pallas_call | solution.py:635
  118.9 0.0 copy-start.1
  118.9 1.9 %pad_maximum_fusion = bf16[4,136,2048]{2,1,0:T(8,128)(2,1)S(1)} fusion(bf16[4,128,2048]{2,1,0:T(8,128)(2,1)} %get-tuple-element.11, bf16[4,8,2048]{2,1,0:T(8,128)(2,1)} %get-tuple-element.10), kind=kLoop, calls=%fused_computation | loop fusion | flops 4456448 | bytes 4456448 | tf_op jit(solution)/shard_map/concatenate | solution.py:673
  120.8 0.7 copy-done.1
  121.5 0.0 copy-start
  121.5 1.9 %convolution_convert_fusion = bf16[544,768]{1,0:T(8,128)(2,1)S(1)} fusion(bf16[544,2048]{1,0:T(8,128)(2,1)S(1)} %bitcast.10, bf16[2048,768]{1,0:T(8,128)(2,1)S(1)} %copy-done.1), kind=kOutput, calls=%fused_computation.7 | convolution fusion | flops 1711693824 | bytes 6209536 | tf_op jit(solution)/shard_map/dot_general | solution.py:674
  123.4 0.0 copy-done
  123.4 1.9 %convolution_convert_fusion.1 = bf16[544,768]{1,0:T(8,128)(2,1)S(1)} fusion(bf16[544,2048]{1,0:T(8,128)(2,1)S(1)} %bitcast.11, bf16[2048,768]{1,0:T(8,128)(2,1)S(1)} %copy-done), kind=kOutput, calls=%fused_computation.8 | convolution fusion | flops 1711693824 | bytes 6209536 | tf_op jit(solution)/shard_map/dot_general | solution.py:675
  125.3 0.1 convert.1
  125.4 0.9 dynamic-slice_reduce_fusion.2
  126.3 1.8 %broadcast_select_fusion.hidden = bf16[4,128,768]{2,1,0:T(8,128)(2,1)} fusion(pred[768]{0:T(1024)(128)(4,1)S(1)} %iota_compare_fusion, bf16[4,136,768]{2,1,0:T(8,128)(2,1)S(1)} %bitcast.13, f32[4,136,768]{2,1,0:T(8,128)S(1)} %convert.1, f32[768]{0:T(1024)S(1)} %get-tuple-element.17, f32[768]{0:T(1024)S(1)} %get-tuple-element.16, f32[768]{0:T(1024)S(1)} %get-tuple-element.15), kind=kLoop, calls=%fused_computation.9 | loop fusion | flops 5111808 | bytes 6301440 | tf_op jit(solution)/shard_map/jit(_where)/select_n | solution.py:685
  128.1 26.6 %down.1 = bf16[64,2048]{1,0:T(8,128)(2,1)} custom-call(bf16[4,128,768]{2,1,0:T(8,128)(2,1)} %broadcast_select_fusion.hidden, bf16[2816,2048]{1,0:T(8,128)(2,1)} %weight.1, f32[64,2048]{1,0:T(8,128)} %get-tuple-element.14.stream), custom_call_target="tpu_custom_call" | custom-call | tf_op jit(solution)/shard_map/down/pallas_call | solution.py:687
  154.7 1.7 %copy.16 = bf16[64,2048]{1,0:T(8,128)(2,1)} copy(bf16[64,2048]{1,0:T(8,128)(2,1)} %down.1) | data formatting | bytes 524288
  (1 shorter events, 0.0 us)
Async XLA Ops:
  118.9 2.6 %copy-start.1 = (bf16[2048,768]{1,0:T(8,128)(2,1)S(1)}, bf16[2048,768]{1,0:T(8,128)(2,1)}, u32[]{:S(2)}) copy-start(bf16[2048,768]{1,0:T(8,128)(2,1)} %get-tuple-element.13) | copy-start | bytes 9437188
  121.5 1.9 %copy-start = (bf16[2048,768]{1,0:T(8,128)(2,1)S(1)}, bf16[2048,768]{1,0:T(8,128)(2,1)}, u32[]{:S(2)}) copy-start(bf16[2048,768]{1,0:T(8,128)(2,1)} %get-tuple-element.12) | copy-start | bytes 9437188

commit v6 on v4

--- a/solution.py
+++ b/solution.py
@@ -231,7 +231,14 @@
     def send_weights(early):
         for d in range(planes - 1, 0, -1):
 
-            @pl.when((z + d >= planes) if early else (z + d < planes))
+            if d == planes - 1:
+                turn = (z > 0) if early else None
+            else:
+                turn = (z + d >= planes) if early else (z + d < planes)
+            if turn is None:
+                continue
+
+            @pl.when(turn)
             def _():
                 for copy in lanes[d]:
                     copy.start()
@@ -306,6 +313,11 @@
         def _():
             block = keys_of(z, e)
             remote(block, block, kv_send.at[1, e], kv_recv.at[1, e], above, tp).start()
+
+    @pl.when(z == 0)
+    def _():
+        for copy in lanes[planes - 1]:
+            copy.start()
 
     for copy in own[3:]:
         copy.wait()

time: 152 us -> 152 us (level)
  no operation moved by 1% of the time
where the time goes in v6:
time: 152 us
  Pallas kernels  141 us (93%)
  matrix products  3.81 us (3%)
  other arithmetic  3.8 us (2%)
  local copies, waits for them, and re-layouts  3.25 us (2%)
    pallas_call x1, Pallas kernels, shorter_routes(): pl.pallas_call(functools.partial(front_kernel, plane, planes, width), out...  114 us
    pallas_call x1, Pallas kernels, shorter_routes(): pl.pallas_call(functools.partial(down_kernel, plane, planes, starts), out...  26.6 us

profile of v6, /device:TPU:25, one launch (start us, length us, event | category | flops | bytes accessed | tf_op | source)
XLA Modules:
  0.0 151.7 jit_solution(11824747581877721646)
XLA Ops:
  0.0 114.2 %front.1 = (bf16[2048,768]{1,0:T(8,128)(2,1)}, bf16[2048,768]{1,0:T(8,128)(2,1)}, bf16[4,128,2048]{2,1,0:T(8,128)(2,1)}, bf16[4,8,2048]{2,1,0:T(8,128)(2,1)}, f32[64,2048]{1,0:T(8,128)}) custom-call(bf16[128,512]{1,0:T(8,128)(2,1)} %q1.1, bf16[128,512]{1,0:T(8,128)(2,1)} %k1.1, bf16[128,512]{1,0:T(8,128)(2,1)} %q2.1, bf16[128,512]{1,0:T(8,128)(2,1)} %k2.1, ...), custom_call_target="tpu_custom_call" | custom-call | tf_op jit(solution)/shard_map/front/pallas_call | solution.py:628
  114.2 0.0 copy-start.1
  114.2 1.9 %pad_maximum_fusion = bf16[4,136,2048]{2,1,0:T(8,128)(2,1)S(1)} fusion(bf16[4,128,2048]{2,1,0:T(8,128)(2,1)} %get-tuple-element.11, bf16[4,8,2048]{2,1,0:T(8,128)(2,1)} %get-tuple-element.10), kind=kLoop, calls=%fused_computation | loop fusion | flops 4456448 | bytes 4456448 | tf_op jit(solution)/shard_map/concatenate | solution.py:666
  116.1 0.7 copy-done.1
  116.8 0.0 copy-start
  116.8 1.9 %convolution_convert_fusion = bf16[544,768]{1,0:T(8,128)(2,1)S(1)} fusion(bf16[544,2048]{1,0:T(8,128)(2,1)S(1)} %bitcast.10, bf16[2048,768]{1,0:T(8,128)(2,1)S(1)} %copy-done.1), kind=kOutput, calls=%fused_computation.7 | convolution fusion | flops 1711693824 | bytes 6209536 | tf_op jit(solution)/shard_map/dot_general | solution.py:667
  118.7 0.0 copy-done
  118.7 1.9 %convolution_convert_fusion.1 = bf16[544,768]{1,0:T(8,128)(2,1)S(1)} fusion(bf16[544,2048]{1,0:T(8,128)(2,1)S(1)} %bitcast.11, bf16[2048,768]{1,0:T(8,128)(2,1)S(1)} %copy-done), kind=kOutput, calls=%fused_computation.8 | convolution fusion | flops 1711693824 | bytes 6209536 | tf_op jit(solution)/shard_map/dot_general | solution.py:668
  120.6 0.1 convert.1
  120.7 0.9 dynamic-slice_reduce_fusion.2
  121.7 1.8 %broadcast_select_fusion.hidden = bf16[4,128,768]{2,1,0:T(8,128)(2,1)} fusion(pred[768]{0:T(1024)(128)(4,1)S(1)} %iota_compare_fusion, bf16[4,136,768]{2,1,0:T(8,128)(2,1)S(1)} %bitcast.13, f32[4,136,768]{2,1,0:T(8,128)S(1)} %convert.1, f32[768]{0:T(1024)S(1)} %get-tuple-element.17, f32[768]{0:T(1024)S(1)} %get-tuple-element.16, f32[768]{0:T(1024)S(1)} %get-tuple-element.15), kind=kLoop, calls=%fused_computation.9 | loop fusion | flops 5111808 | bytes 6301440 | tf_op jit(solution)/shard_map/jit(_where)/select_n | solution.py:678
  123.4 26.6 %down.1 = bf16[64,2048]{1,0:T(8,128)(2,1)} custom-call(bf16[4,128,768]{2,1,0:T(8,128)(2,1)} %broadcast_select_fusion.hidden, bf16[2816,2048]{1,0:T(8,128)(2,1)} %weight.1, f32[64,2048]{1,0:T(8,128)} %get-tuple-element.14.stream), custom_call_target="tpu_custom_call" | custom-call | tf_op jit(solution)/shard_map/down/pallas_call | solution.py:680
  150.0 1.7 %copy.16 = bf16[64,2048]{1,0:T(8,128)(2,1)} copy(bf16[64,2048]{1,0:T(8,128)(2,1)} %down.1) | data formatting | bytes 524288
  (1 shorter events, 0.0 us)
Async XLA Ops:
  114.2 2.6 %copy-start.1 = (bf16[2048,768]{1,0:T(8,128)(2,1)S(1)}, bf16[2048,768]{1,0:T(8,128)(2,1)}, u32[]{:S(2)}) copy-start(bf16[2048,768]{1,0:T(8,128)(2,1)} %get-tuple-element.13) | copy-start | bytes 9437188
  116.8 1.9 %copy-start = (bf16[2048,768]{1,0:T(8,128)(2,1)S(1)}, bf16[2048,768]{1,0:T(8,128)(2,1)}, u32[]{:S(2)}) copy-start(bf16[2048,768]{1,0:T(8,128)(2,1)} %get-tuple-element.12) | copy-start | bytes 9437188
